TPU v7x, 32 devices: a whole 2x2x4 slice. The times are simulated.
32 devices in a mesh: grp: 2 (over y), sp: 4 (over z), tp: 4 (over x, core).
Axes of the slice: x: 2, y: 2, z: 4, core: 2. Of those that a mesh axis runs over, the one named last changes fastest.
Arguments:
- residual: bfloat16 [2048, 2048], P(('grp', 'sp')), parts along dimension 0, may hold values from -34 to 34
- queries: bfloat16 [2048, 1024], P(('grp', 'sp'), 'tp'), parts along dimension 0, may hold values from -400 to 400
- keys: bfloat16 [2048, 512], P(('grp', 'sp'), 'tp'), parts along dimension 0, may hold values from -8 to 8
- values: bfloat16 [2048, 512], P(('grp', 'sp'), 'tp'), parts along dimension 0, may hold values from -6 to 6
- segments: int32 [2048], P(('grp', 'sp')), parts along dimension 0, may hold values from 0 to 2, never falling along the last dimension, each value on 1 to 768 neighbouring positions
- routes: int32 [2048, 2], P(('grp', 'sp')), parts along dimension 0, may hold values from 0 to 3, all different within a row; in each aligned block of 256 rows (0 to 255, 256 to 511, ...) at most 256 rows name the same one
- route_weight: float32 [2048, 2], P(('grp', 'sp')), parts along dimension 0, may hold values from 0.3 to 3
- sinks: float32 [16], P('tp'), may hold values from 1 to 6
- out_weight: bfloat16 [1024, 2048], P('tp'), may hold values from -1 to 1
- norm_gain: float32 [2048], replicated, may hold values from 0.1 to 1.9
- expert_gate: bfloat16 [4, 2048, 1024], P('sp', None, 'tp'), may hold values from -0.125 to 0.125
- expert_up: bfloat16 [4, 2048, 1024], P('sp', None, 'tp'), may hold values from -0.125 to 0.125
- expert_down: bfloat16 [4, 1024, 2048], P('sp', None, 'tp'), may hold values from -0.1875 to 0.1875
- shared_gate: bfloat16 [2048, 1024], P(None, 'tp'), may hold values from -0.125 to 0.125
- shared_up: bfloat16 [2048, 1024], P(None, 'tp'), may hold values from -0.125 to 0.125
- shared_down: bfloat16 [1024, 2048], P(None, 'tp'), may hold values from -0.1875 to 0.1875
Outputs:
- mixed: bfloat16 [2048, 2048], P(('grp', 'sp'), 'tp'), parts along dimension 0
There are 2 independent parts, one for each index of `grp`. A program takes and returns all parts, laid end to end along the dimension named above; an argument that names none is the same for every part. Nothing has to cross between parts.
Inputs may be any that keep to these rules, and one draw needn't show every extreme that they name: `routes`: each row names 2 different experts. In the rows of one device no expert is named by more than 256 rows, and in some device's rows an expert is named by exactly 256. `segments`: document numbers never fall along the positions; every document spans 1 to 768 positions and one spans exactly 768.
All inputs are finite; a program needn't handle non-finite values.
Results may differ from a plain program's by a relative error of at most 0.0065.
Values may be sent and summed in bfloat16 or wider, within the bound.
No kernel may reach another device: no remote copies, remote signals or barrier semaphores. Data moves between devices by JAX's collectives and lax.ppermute only.
A program may use at most 64 MiB of HBM per device.

v0:
```python
import functools

import jax
import jax.numpy as jnp
from jax import lax
from jax.experimental import pallas as pl
from jax.experimental.pallas import tpu as pltpu
from jax.sharding import PartitionSpec as P


HEAD_DIM = 64
WINDOW = 128


epsilon = 1e-06


def passed_along(value, axis, steps):
    count = lax.axis_size(axis)
    leading, last = (max(0, -steps), min(count, count - steps))
    return lax.ppermute(value, axis, [(source, source + steps) for source in range(leading, last)])


def banded(prev_rows, own_rows, window_len):
    blocks = own_rows.shape[0] // window_len
    joined = jnp.concatenate([prev_rows, own_rows], axis=0)
    shaped = joined.reshape((blocks + 1, window_len) + own_rows.shape[1:])
    return jnp.concatenate([shaped[:-1], shaped[1:]], axis=1)


KERNEL_VMEM = 16 * 2**20


def swapped(value, axis, bit):
    count = lax.axis_size(axis)
    return lax.ppermute(value, axis, [(source, source ^ bit) for source in range(count)])


def gathered(value):
    pieces = {0: value}
    bit = lax.axis_size("tp") // 2
    while bit:
        more = {}
        for known, held in pieces.items():
            more[known ^ bit] = swapped(held, "tp", bit)
        pieces.update(more)
        bit //= 2
    return [pieces[j] for j in range(len(pieces))]


def dot32(left, right):
    return jnp.dot(left, right, preferred_element_type=jnp.float32)


def columns(ref, spot):
    width = ref.shape[1] // lax.axis_size("tp")
    return ref[:, pl.ds(pl.multiple_of(spot * width, width), width)]


def column(row):
    return jnp.transpose(jnp.broadcast_to(row, (8, row.shape[1])))[:, :1]


def prologue_kernel(place_ref, marks_ref, k_ref, v_ref, out_ref, packed_ref, *part_refs):
    span, rows = WINDOW, k_ref.shape[0]
    tail = slice(rows - span, rows)
    packed_ref[:span, :] = k_ref[tail, :]
    packed_ref[span : 2 * span, :] = v_ref[tail, :]
    marks = jnp.broadcast_to(marks_ref[:, tail], (packed_ref.shape[0] - 2 * span, span))
    packed_ref[2 * span :, :] = marks.astype(jnp.bfloat16)
    for j, part_ref in enumerate(part_refs, 1):
        part_ref[...] = columns(out_ref, place_ref[0] ^ j)


def attend_kernel(sink_ref, row_ref, q_ref, k_ref, v_ref, halo_ref, out_ref):
    span = WINDOW
    rows = q_ref.shape[0]
    kv_local = k_ref.shape[1] // HEAD_DIM
    group_size = q_ref.shape[1] // k_ref.shape[1]
    halo = halo_ref[...]
    keys = jnp.concatenate([halo[:span], k_ref[...]], axis=0)
    values = jnp.concatenate([halo[span : 2 * span], v_ref[...]], axis=0)
    own = row_ref[...]
    marks = jnp.concatenate([halo[2 * span : 2 * span + 1].astype(jnp.float32), own], axis=1)
    down_marks = column(own)
    place = lax.broadcasted_iota(jnp.int32, (span, 2 * span), 0)
    offsets = place + span - lax.broadcasted_iota(jnp.int32, (span, 2 * span), 1)
    near = (offsets >= 0) & (offsets < span)
    for block in range(rows // span):
        low = block * span
        allowed = near & (down_marks[low : low + span] == marks[:, low : low + 2 * span])
        outs = []
        for kv in range(kv_local):
            lanes = slice(kv * HEAD_DIM, (kv + 1) * HEAD_DIM)
            key_part = keys[low : low + 2 * span, lanes]
            value_part = values[low : low + 2 * span, lanes]
            for member in range(group_size):
                head = kv * group_size + member
                query = q_ref[low : low + span, head * HEAD_DIM : (head + 1) * HEAD_DIM]
                scores = lax.dot_general(
                    query, key_part, (((1,), (1,)), ((), ())), preferred_element_type=jnp.float32
                ) * HEAD_DIM ** (-0.5)
                sink = sink_ref[head]
                masked = jnp.where(allowed, scores, -jnp.inf)
                top = jnp.maximum(jnp.max(masked, axis=1, keepdims=True), sink)
                terms = jnp.exp(masked - top)
                total = jnp.sum(terms, axis=1, keepdims=True) + jnp.exp(sink - top)
                probs = (terms / total).astype(jnp.bfloat16)
                outs.append(dot32(probs, value_part).astype(jnp.bfloat16))
        out_ref[low : low + span, :] = jnp.concatenate(outs, axis=1)


def update_kernel(count, place_ref, residual_ref, weight_ref, *refs):
    acts, parts, out_ref = refs[:count], refs[count:-1], refs[-1]
    place = place_ref[0]
    total = columns(residual_ref, place).astype(jnp.float32)
    total = total + dot32(acts[0][...], columns(weight_ref, place))
    for act, part in zip(acts[1:], parts, strict=True):
        total = total + dot32(act[...], part[...])
    out_ref[...] = total.astype(jnp.bfloat16)


def hidden_kernel(count, pairs, place_ref, gain_ref, *refs):
    pieces, weights, out_ref = refs[:count], refs[count:-1], refs[-1]
    place = place_ref[0]
    width = sum(piece.shape[1] for piece in pieces)
    hidden = weights[0].shape[2]
    squares = 0.0
    for piece in pieces:
        rows = piece[...].astype(jnp.float32)
        squares = squares + jnp.sum(rows * rows, axis=1, keepdims=True)
    scale = lax.rsqrt(squares / width + epsilon)
    sums = [None] * (2 * pairs)
    for j in range(count):
        at = place ^ j
        normed = (pieces[j][...].astype(jnp.float32) * scale * gain_ref[at]).astype(jnp.bfloat16)
        for n in range(2 * pairs):
            term = dot32(normed, weights[n][at])
            sums[n] = term if j == 0 else sums[n] + term
    for n in range(pairs):
        gate, lin = sums[2 * n], sums[2 * n + 1]
        act = gate / (1.0 + jnp.exp(-gate)) * lin
        out_ref[:, n * hidden : (n + 1) * hidden] = act.astype(jnp.bfloat16)


def down_kernel(count, place_ref, down_ref, *refs):
    place = place_ref[0]
    total = dot32(refs[0][...], down_ref[place])
    for j in range(1, count):
        total = total + dot32(refs[j][...], down_ref[place ^ j])
    refs[-1][...] = total.astype(jnp.bfloat16)


def weights_of(spot, routes_ref, weight_ref, steps):
    routes, weight = routes_ref[...], weight_ref[...]
    rows = []
    for k in range(steps):
        named = jnp.where(routes == (spot ^ k), weight, 0.0)
        rows.append(jnp.sum(named, axis=0, keepdims=True))
    rows += [jnp.zeros_like(rows[0])] * (-steps % 8)
    return jnp.transpose(jnp.concatenate(rows, axis=0))


def own_kernel(count, place_ref, routes_ref, weight_ref, down_ref, shared_ref, updated_ref, *refs):
    place = place_ref[0]
    hidden = down_ref.shape[1]
    for j in range(count):
        terms = [
            dot32(refs[j][:, :hidden], down_ref[place ^ j]),
            dot32(refs[j][:, hidden:], shared_ref[place ^ j]),
        ]
        sums = terms if j == 0 else [old + term for old, term in zip(sums, terms, strict=True)]
    weight = weights_of(place_ref[1], routes_ref, weight_ref, 1)[:, :1]
    routed = sums[0].astype(jnp.bfloat16).astype(jnp.float32)
    refs[-1][...] = updated_ref[...].astype(jnp.float32) + sums[1] + routed * weight


def mix_kernel(count, place_ref, routes_ref, weight_ref, base_ref, *refs):
    weights = weights_of(place_ref[1], routes_ref, weight_ref, count + 1)
    total = base_ref[...]
    for k in range(count):
        total = total + refs[k][...].astype(jnp.float32) * weights[:, k + 1 : k + 2]
    refs[-1][...] = total.astype(jnp.bfloat16)


def call(kernel, out, args, scalars=1):
    specs = [pl.BlockSpec(memory_space=pltpu.SMEM if n < scalars else pltpu.VMEM) for n in range(len(args))]
    vmem = pl.BlockSpec(memory_space=pltpu.VMEM)
    return pl.pallas_call(
        kernel,
        out_shape=out,
        in_specs=specs,
        out_specs=[vmem] * len(out) if isinstance(out, list) else vmem,
        compiler_params=pltpu.CompilerParams(vmem_limit_bytes=KERNEL_VMEM),
    )(*args)


def dense_shards(*args):
    return dense_steps(*args)


def dense_steps(
    residual,
    queries,
    keys,
    values,
    segments,
    routes,
    route_weight,
    sinks,
    out_weight,
    norm_gain,
    expert_gate,
    expert_up,
    expert_down,
    shared_gate,
    shared_up,
    shared_down,
):
    rows_here, model_width = residual.shape
    tp_count, sp_count = lax.axis_size("tp"), lax.axis_size("sp")
    tp_index = lax.axis_index("tp").astype(jnp.int32)
    sp_index = lax.axis_index("sp").astype(jnp.int32)
    place = jnp.stack([tp_index, sp_index])
    span = WINDOW
    col_width = model_width // tp_count
    heads_width = out_weight.shape[0]
    bf16, f32 = jnp.bfloat16, jnp.float32
    shape = jax.ShapeDtypeStruct

    own_marks = (segments % 256 + 1).astype(f32)[None, :]
    packed, *parts = call(
        prologue_kernel,
        [shape((2 * span + 16, span), bf16)] + [shape((heads_width, col_width), bf16)] * (tp_count - 1),
        [place, own_marks, keys, values, out_weight],
    )
    halo = passed_along(packed, "sp", 1)
    parts = [swapped(part, "tp", j) for j, part in enumerate(parts, 1)]
    attended = call(
        attend_kernel, shape(queries.shape, bf16), [sinks, own_marks, queries, keys, values, halo]
    )
    own = call(
        functools.partial(update_kernel, tp_count),
        shape((rows_here, col_width), bf16),
        [place, residual, out_weight, *gathered(attended), *parts],
    )

    gain = norm_gain.reshape(tp_count, 1, col_width)
    gate, up, common_gate, common_up = [
        weight.reshape(tp_count, col_width, -1) for weight in (expert_gate, expert_up, shared_gate, shared_up)
    ]
    hidden = gate.shape[2]
    down, common_down = [weight.reshape(tp_count, hidden, col_width) for weight in (expert_down, shared_down)]
    routes, route_weight = routes.T, route_weight.T
    cols = (rows_here, col_width)

    blocks = [own] + [swapped(own, "sp", k) for k in range(1, sp_count - 1)]
    blocks.append(swapped(blocks[(sp_count - 1) ^ 1], "sp", 1))
    returned = []
    base = None
    for k in range(sp_count):
        pieces = gathered(blocks[k])
        pairs = 2 if k == 0 else 1
        weights = [gate, up, common_gate, common_up][: 2 * pairs]
        act = call(
            functools.partial(hidden_kernel, tp_count, pairs),
            shape((rows_here, pairs * hidden), bf16),
            [place, gain, *pieces, *weights],
        )
        acts = gathered(act)
        if k == 0:
            base = call(
                functools.partial(own_kernel, tp_count),
                shape(cols, f32),
                [place, routes, route_weight, down, common_down, own, *acts],
            )
        else:
            out = call(
                functools.partial(down_kernel, tp_count), shape(cols, bf16), [place, down, *acts]
            )
            returned.append(swapped(out, "sp", k))
    return call(
        functools.partial(mix_kernel, sp_count - 1),
        shape(cols, bf16),
        [place, routes, route_weight, base, *returned],
    )


def shards(
    residual,
    queries,
    keys,
    values,
    segments,
    routes,
    route_weight,
    sinks,
    out_weight,
    norm_gain,
    expert_gate,
    expert_up,
    expert_down,
    shared_gate,
    shared_up,
    shared_down,
):
    rows_here = residual.shape[0]
    model_width = residual.shape[1]
    tp_count = lax.axis_size("tp")
    tp_index = lax.axis_index("tp")
    head_local = queries.shape[1] // HEAD_DIM
    kv_local = keys.shape[1] // HEAD_DIM
    group_size = head_local // kv_local
    window_len = WINDOW
    blocks = rows_here // window_len
    own_marks = (segments % 256 + 1).astype(jnp.bfloat16)
    prev_keys, prev_values, prev_marks = passed_along(
        (
            keys[rows_here - window_len :],
            values[rows_here - window_len :],
            own_marks[rows_here - window_len :],
        ),
        "sp",
        1,
    )
    key_band = banded(prev_keys, keys, window_len).reshape(
        blocks, 2 * window_len, kv_local, HEAD_DIM
    )
    value_band = banded(prev_values, values, window_len).reshape(
        blocks, 2 * window_len, kv_local, HEAD_DIM
    )
    mark_band = banded(prev_marks, own_marks, window_len).astype(jnp.float32)
    query_marks = own_marks.reshape(blocks, window_len).astype(jnp.float32)
    query_blocks = queries.reshape(blocks, window_len, kv_local, group_size, HEAD_DIM)
    scores = jnp.einsum(
        "nqhgd,nkhd->nhgqk", query_blocks, key_band, preferred_element_type=jnp.float32
    ) * HEAD_DIM ** (-0.5)
    offsets = jnp.arange(window_len)[:, None] + window_len - jnp.arange(2 * window_len)[None, :]
    allowed = (
        (offsets >= 0) & (offsets < window_len) & (query_marks[:, :, None] == mark_band[:, None, :])
    )
    sink_logits = sinks.reshape(kv_local, group_size)[None, :, :, None]
    masked = jnp.where(allowed[:, None, None], scores, -jnp.inf)
    top_score = jnp.maximum(jnp.max(masked, axis=-1), sink_logits)
    exp_terms = jnp.where(allowed[:, None, None], jnp.exp(scores - top_score[..., None]), 0.0)
    denominator = jnp.sum(exp_terms, axis=-1) + jnp.exp(sink_logits - top_score)
    probabilities = (exp_terms / denominator[..., None]).astype(jnp.bfloat16)
    attended = jnp.einsum(
        "nhgqk,nkhd->nqhgd", probabilities, value_band, preferred_element_type=jnp.float32
    )
    attended = attended.astype(jnp.bfloat16).reshape(rows_here, head_local * HEAD_DIM)
    partial_value = jnp.dot(attended, out_weight, preferred_element_type=jnp.float32)
    col_width = model_width // tp_count
    col_start = tp_index * col_width
    summed = lax.psum(partial_value, "tp")
    updated = (residual.astype(jnp.float32) + summed).astype(jnp.bfloat16)
    updated_f32 = updated.astype(jnp.float32)
    inv_rms = lax.rsqrt(jnp.mean(updated_f32 * updated_f32, axis=-1, keepdims=True) + epsilon)
    normed = (updated_f32 * inv_rms * norm_gain).astype(jnp.bfloat16)
    updated_cols = lax.dynamic_slice_in_dim(updated, col_start, col_width, 1)
    normed_cols = lax.dynamic_slice_in_dim(normed, col_start, col_width, 1)
    shared_pre = jnp.dot(normed, shared_gate, preferred_element_type=jnp.float32)
    shared_lin = jnp.dot(normed, shared_up, preferred_element_type=jnp.float32)
    shared_act = (jax.nn.silu(shared_pre) * shared_lin).astype(jnp.bfloat16)
    top_count = routes.shape[1]
    experts = lax.axis_size("sp")
    capacity = 2 * rows_here * top_count // experts
    flat_ids = routes.reshape(-1)
    one_hot = (flat_ids[:, None] == jnp.arange(experts, dtype=jnp.int32)[None, :]).astype(jnp.int32)
    rank_in = jnp.cumsum(one_hot, axis=0) - one_hot
    slot_dest = flat_ids * capacity + jnp.sum(rank_in * one_hot, axis=1)
    token_of = jnp.arange(rows_here * top_count, dtype=jnp.int32) // top_count
    slot_token = jnp.full((experts * capacity,), -1, jnp.int32).at[slot_dest].set(token_of)
    filled = slot_token >= 0
    safe_token = jnp.where(filled, slot_token, 0)
    outgoing = jnp.where(filled[:, None], normed_cols[safe_token], jnp.zeros((), jnp.bfloat16))
    pieces = lax.all_to_all(
        outgoing.reshape(experts, capacity, col_width),
        "sp",
        split_axis=0,
        concat_axis=0,
        tiled=True,
    )
    arrived = lax.all_gather(pieces, "tp", axis=2, tiled=True)
    expert_rows = arrived.reshape(-1, model_width)
    gate_pre = jnp.dot(expert_rows, expert_gate[0], preferred_element_type=jnp.float32)
    up_lin = jnp.dot(expert_rows, expert_up[0], preferred_element_type=jnp.float32)
    expert_act = (jax.nn.silu(gate_pre) * up_lin).astype(jnp.bfloat16)
    gathered_expert, gathered_shared = (
        lax.all_gather(expert_act, "tp", axis=1, tiled=True),
        lax.all_gather(shared_act, "tp", axis=1, tiled=True),
    )
    expert_out = jnp.dot(
        gathered_expert, expert_down[0], preferred_element_type=jnp.float32
    ).astype(jnp.bfloat16)
    returned = lax.all_to_all(
        expert_out.reshape(experts, capacity, col_width),
        "sp",
        split_axis=0,
        concat_axis=0,
        tiled=True,
    )
    returned = returned.reshape(experts * capacity, col_width)
    picked = returned[slot_dest].astype(jnp.float32).reshape(rows_here, top_count, col_width)
    routed = jnp.sum(picked * route_weight[:, :, None], axis=1)
    shared_cols = jnp.dot(gathered_shared, shared_down, preferred_element_type=jnp.float32)
    return (updated_cols.astype(jnp.float32) + shared_cols + routed).astype(jnp.bfloat16)


def is_dense(rows_here, kv_width, top_count, sizes):
    experts, tp_count = sizes["sp"], sizes["tp"]
    dense = 2 * rows_here * top_count // experts >= rows_here
    even = experts & (experts - 1) == 0 and tp_count & (tp_count - 1) == 0
    return dense and even and kv_width // tp_count == WINDOW and rows_here % WINDOW == 0


def choose(*args):
    sizes = {axis: lax.axis_size(axis) for axis in ("sp", "tp")}
    dense = is_dense(args[0].shape[0], args[2].shape[1] * sizes["tp"], args[5].shape[1], sizes)
    return (dense_shards if dense else shards)(*args)


def solution(mesh):
    placed = (
        P(("grp", "sp"), None),
        P(("grp", "sp"), "tp"),
        P(("grp", "sp"), "tp"),
        P(("grp", "sp"), "tp"),
        P(("grp", "sp")),
        P(("grp", "sp"), None),
        P(("grp", "sp"), None),
        P("tp"),
        P("tp", None),
        P(),
        P("sp", None, "tp"),
        P("sp", None, "tp"),
        P("sp", None, "tp"),
        P(None, "tp"),
        P(None, "tp"),
        P(None, "tp"),
    )
    return jax.shard_map(
        choose, mesh=mesh, in_specs=placed, out_specs=P(("grp", "sp"), "tp"), check_vma=False
    )
```

profile of v0, /device:TPU:10, one launch (start us, length us, event | category | flops | bytes accessed | tf_op | source)
XLA Modules:
  0.0 114.1 jit_solution(10834477801306483853)
XLA Ops:
  0.0 0.7 copy-done.18
  0.7 0.1 pad_add_fusion.place_ref
  0.8 1.2 %copy-done.3 = bf16[256,2048]{1,0:T(8,128)(2,1)S(1)} copy-done((bf16[256,2048]{1,0:T(8,128)(2,1)S(1)}, bf16[256,2048]{1,0:T(8,128)(2,1)}, u32[]{:S(2)}) %copy-start.3) | copy-done | bytes 1048600
  2.0 0.8 copy-done.9
  2.8 0.8 copy-done.11
  3.7 0.6 shard_map.154
  4.3 3.5 %collective-permute-start = (bf16[272,128]{1,0:T(8,128)(2,1)S(1)}, bf16[272,128]{1,0:T(8,128)(2,1)S(1)}, u32[]{:S(2)}, u32[]{:S(2)}) collective-permute-start(bf16[272,128]{1,0:T(8,128)(2,1)S(1)} %get-tuple-element.9), channel_id=1, source_target_pairs={{0,4},{4,8},{8,12},{1,5},{5,9},{9,13},{2,6},{6,10},{10,14},{3,7},{... | collective-permute-start | bytes 208904 | tf_op jit(solution)/shard_map/ppermute | solution.py:21
  7.8 0.1 collective-permute-start.4
  7.9 0.0 copy-start.17
  7.9 0.6 collective-permute-start.5
  8.5 1.2 %collective-permute-start.6 = (bf16[256,512]{1,0:T(8,128)(2,1)S(1)}, bf16[256,512]{1,0:T(8,128)(2,1)S(1)}, u32[]{:S(2)}, u32[]{:S(2)}) collective-permute-start(bf16[256,512]{1,0:T(8,128)(2,1)S(1)} %get-tuple-element.12), channel_id=1, source_target_pairs={{0,3},{1,2},{2,1},{3,0},{4,7},{5,6},{6,5},{7,4},{8,11},{9,10},{10,... | collective-permute-start | bytes 786440 | tf_op jit(solution)/shard_map/ppermute | solution.py:36
  9.7 0.8 collective-permute-done.halo_ref
  10.5 0.0 copy-start.14
  10.5 0.9 copy-done.14
  11.4 2.0 %shard_map.155.refs_0_ = bf16[256,256]{1,0:T(8,128)(2,1)S(1)} custom-call(f32[4]{0:T(128)S(1)} %copy-done.17, f32[1,256]{1,0:T(1,128)S(1)} %bitcast.32, bf16[256,256]{1,0:T(8,128)(2,1)S(1)} %copy-done.14, bf16[256,128]{1,0:T(8,128)(2,1)S(1)} %copy-done.10, bf16[256,128]{1,0:T(8,128)(2,1)S(1)} %copy-done.12, bf16[272,128]{1,0:T(8,128)(2,1)S(1)} %collective-permute-done.halo_ref), custom_call_target="tpu_custom_call" | custom-call | tf_op jit(solution)/shard_map/pallas_call | solution.py:189
  13.4 0.6 collective-permute-start.2
  14.0 11.0 %collective-permute-done.2.refs_2_ = bf16[256,256]{1,0:T(8,128)(2,1)S(1)} collective-permute-done((bf16[256,256]{1,0:T(8,128)(2,1)S(1)}, bf16[256,256]{1,0:T(8,128)(2,1)S(1)}, u32[]{:S(2)}, u32[]{:S(2)}) %collective-permute-start.2) | collective-permute-done | bytes 131104 | tf_op jit(solution)/shard_map/ppermute | solution.py:36
  25.0 1.3 %collective-permute-done.3.refs_3_ = bf16[256,256]{1,0:T(8,128)(2,1)S(1)} collective-permute-done((bf16[256,256]{1,0:T(8,128)(2,1)S(1)}, bf16[256,256]{1,0:T(8,128)(2,1)S(1)}, u32[]{:S(2)}, u32[]{:S(2)}) %collective-permute-start.3) | collective-permute-done | bytes 131104 | tf_op jit(solution)/shard_map/ppermute | solution.py:36
  26.3 1.2 %copy-done.6 = bf16[256,2048]{1,0:T(8,128)(2,1)S(1)} copy-done((bf16[256,2048]{1,0:T(8,128)(2,1)S(1)}, bf16[256,2048]{1,0:T(8,128)(2,1)}, u32[]{:S(2)}) %copy-start.6) | copy-done | bytes 1048600
  27.6 1.0 shard_map.156.refs_0_.updated_ref
  28.6 0.5 collective-permute-start.21
  29.0 2.6 %collective-permute-start.13 = (bf16[256,512]{1,0:T(8,128)(2,1)S(1)}, bf16[256,512]{1,0:T(8,128)(2,1)S(1)}, u32[]{:S(2)}, u32[]{:S(2)}) collective-permute-start(bf16[256,512]{1,0:T(8,128)(2,1)S(1)} %shard_map.156.refs_0_.updated_ref), channel_id=1, source_target_pairs={{0,4},{4,0},{8,12},{12,8},{1,5},{5,1},{9,13},{13,9},{2,6},{6,2},{1... | collective-permute-start | bytes 786440 | tf_op jit(solution)/shard_map/ppermute | solution.py:36
  31.7 0.5 collective-permute-start.8
  32.2 8.3 %collective-permute-done.21.refs_0_ = bf16[256,512]{1,0:T(8,128)(2,1)S(1)} collective-permute-done((bf16[256,512]{1,0:T(8,128)(2,1)S(1)}, bf16[256,512]{1,0:T(8,128)(2,1)S(1)}, u32[]{:S(2)}, u32[]{:S(2)}) %collective-permute-start.21) | collective-permute-done | bytes 262176 | tf_op jit(solution)/shard_map/ppermute | solution.py:36
  40.5 3.5 %collective-permute-start.29 = (bf16[256,512]{1,0:T(8,128)(2,1)S(1)}, bf16[256,512]{1,0:T(8,128)(2,1)S(1)}, u32[]{:S(2)}, u32[]{:S(2)}) collective-permute-start(bf16[256,512]{1,0:T(8,128)(2,1)S(1)} %collective-permute-done.21.refs_0_), channel_id=1, source_target_pairs={{0,4},{4,0},{8,12},{12,8},{1,5},{5,1},{9,13},{13,9},{2,6},{6,2},{1... | collective-permute-start | bytes 786440 | tf_op jit(solution)/shard_map/ppermute | solution.py:36
  44.1 0.5 collective-permute-start.15
  44.6 1.5 %collective-permute-start.23 = (bf16[256,512]{1,0:T(8,128)(2,1)S(1)}, bf16[256,512]{1,0:T(8,128)(2,1)S(1)}, u32[]{:S(2)}, u32[]{:S(2)}) collective-permute-start(bf16[256,512]{1,0:T(8,128)(2,1)S(1)} %collective-permute-done.21.refs_0_), channel_id=1, source_target_pairs={{0,2},{1,3},{2,0},{3,1},{4,6},{5,7},{6,4},{7,5},{8,10},{9,11},{10,... | collective-permute-start | bytes 786440 | tf_op jit(solution)/shard_map/ppermute | solution.py:36
  46.1 0.2 collective-permute-start.14
  46.3 3.4 %collective-permute-done.29.refs_0_ = bf16[256,512]{1,0:T(8,128)(2,1)S(1)} collective-permute-done((bf16[256,512]{1,0:T(8,128)(2,1)S(1)}, bf16[256,512]{1,0:T(8,128)(2,1)S(1)}, u32[]{:S(2)}, u32[]{:S(2)}) %collective-permute-start.29) | collective-permute-done | bytes 262176 | tf_op jit(solution)/shard_map/ppermute | solution.py:36
  49.8 0.5 collective-permute-start.31
  50.3 2.9 %collective-permute-done.15.refs_2_ = bf16[256,512]{1,0:T(8,128)(2,1)S(1)} collective-permute-done((bf16[256,512]{1,0:T(8,128)(2,1)S(1)}, bf16[256,512]{1,0:T(8,128)(2,1)S(1)}, u32[]{:S(2)}, u32[]{:S(2)}) %collective-permute-start.15) | collective-permute-done | bytes 262176 | tf_op jit(solution)/shard_map/ppermute | solution.py:36
  53.3 0.5 collective-permute-start.22
  53.8 5.1 %collective-permute-done.23.refs_2_ = bf16[256,512]{1,0:T(8,128)(2,1)S(1)} collective-permute-done((bf16[256,512]{1,0:T(8,128)(2,1)S(1)}, bf16[256,512]{1,0:T(8,128)(2,1)S(1)}, u32[]{:S(2)}, u32[]{:S(2)}) %collective-permute-start.23) | collective-permute-done | bytes 262176 | tf_op jit(solution)/shard_map/ppermute | solution.py:36
  58.9 0.5 collective-permute-start.30
  59.4 3.1 %collective-permute-done.31.refs_2_ = bf16[256,512]{1,0:T(8,128)(2,1)S(1)} collective-permute-done((bf16[256,512]{1,0:T(8,128)(2,1)S(1)}, bf16[256,512]{1,0:T(8,128)(2,1)S(1)}, u32[]{:S(2)}, u32[]{:S(2)}) %collective-permute-start.31) | collective-permute-done | bytes 262176 | tf_op jit(solution)/shard_map/ppermute | solution.py:36
  62.5 1.2 %copy-done.8 = bf16[2048,256]{1,0:T(8,128)(2,1)S(1)} copy-done((bf16[2048,256]{1,0:T(8,128)(2,1)S(1)}, bf16[2048,256]{1,0:T(8,128)(2,1)}, u32[]{:S(2)}) %copy-start.8) | copy-done | bytes 1048600
  63.7 2.1 %shard_map.157.refs_0_ = bf16[256,512]{1,0:T(8,128)(2,1)S(1)} custom-call(s32[2]{0:T(128)S(1)} %pad_add_fusion.place_ref, f32[4,1,512]{2,1,0:T(1,128)S(1)} %bitcast.27, bf16[256,512]{1,0:T(8,128)(2,1)S(1)} %shard_map.156.refs_0_.updated_ref, bf16[256,512]{1,0:T(8,128)(2,1)S(1)} %collective-permute-done.7.refs_1_, ...), custom_call_target="tpu_custom_call" | custom-call | tf_op jit(solution)/shard_map/pallas_call | solution.py:189
  65.8 0.6 collective-permute-start.11
  66.4 1.5 %shard_map.159.refs_0_ = bf16[256,256]{1,0:T(8,128)(2,1)S(1)} custom-call(s32[2]{0:T(128)S(1)} %pad_add_fusion.place_ref, f32[4,1,512]{2,1,0:T(1,128)S(1)} %bitcast.28, bf16[256,512]{1,0:T(8,128)(2,1)S(1)} %collective-permute-done.13.refs_0_, bf16[256,512]{1,0:T(8,128)(2,1)S(1)} %collective-permute-done.14.refs_1_, ...), custom_call_target="tpu_custom_call" | custom-call | tf_op jit(solution)/shard_map/pallas_call | solution.py:189
  67.9 1.6 %collective-permute-start.18 = (bf16[256,256]{1,0:T(8,128)(2,1)S(1)}, bf16[256,256]{1,0:T(8,128)(2,1)S(1)}, u32[]{:S(2)}, u32[]{:S(2)}) collective-permute-start(bf16[256,256]{1,0:T(8,128)(2,1)S(1)} %shard_map.159.refs_0_), channel_id=1, source_target_pairs={{0,2},{1,3},{2,0},{3,1},{4,6},{5,7},{6,4},{7,5},{8,10},{9,11},{10,... | collective-permute-start | bytes 393224 | tf_op jit(solution)/shard_map/ppermute | solution.py:36
  69.5 1.5 %shard_map.161.refs_0_ = bf16[256,256]{1,0:T(8,128)(2,1)S(1)} custom-call(s32[2]{0:T(128)S(1)} %pad_add_fusion.place_ref, f32[4,1,512]{2,1,0:T(1,128)S(1)} %bitcast.29, bf16[256,512]{1,0:T(8,128)(2,1)S(1)} %collective-permute-done.21.refs_0_, bf16[256,512]{1,0:T(8,128)(2,1)S(1)} %collective-permute-done.22.refs_1_, ...), custom_call_target="tpu_custom_call" | custom-call | tf_op jit(solution)/shard_map/pallas_call | solution.py:189
  71.0 0.6 collective-permute-start.26
  71.6 1.5 %shard_map.163.refs_0_ = bf16[256,256]{1,0:T(8,128)(2,1)S(1)} custom-call(s32[2]{0:T(128)S(1)} %pad_add_fusion.place_ref, f32[4,1,512]{2,1,0:T(1,128)S(1)} %bitcast.30, bf16[256,512]{1,0:T(8,128)(2,1)S(1)} %collective-permute-done.29.refs_0_, bf16[256,512]{1,0:T(8,128)(2,1)S(1)} %collective-permute-done.30.refs_1_, ...), custom_call_target="tpu_custom_call" | custom-call | tf_op jit(solution)/shard_map/pallas_call | solution.py:189
  73.1 1.6 %collective-permute-start.34 = (bf16[256,256]{1,0:T(8,128)(2,1)S(1)}, bf16[256,256]{1,0:T(8,128)(2,1)S(1)}, u32[]{:S(2)}, u32[]{:S(2)}) collective-permute-start(bf16[256,256]{1,0:T(8,128)(2,1)S(1)} %shard_map.163.refs_0_), channel_id=1, source_target_pairs={{0,2},{1,3},{2,0},{3,1},{4,6},{5,7},{6,4},{7,5},{8,10},{9,11},{10,... | collective-permute-start | bytes 393224 | tf_op jit(solution)/shard_map/ppermute | solution.py:36
  74.6 0.4 collective-permute-done.11.refs_2_
  75.1 2.8 %collective-permute-done.18.refs_2_ = bf16[256,256]{1,0:T(8,128)(2,1)S(1)} collective-permute-done((bf16[256,256]{1,0:T(8,128)(2,1)S(1)}, bf16[256,256]{1,0:T(8,128)(2,1)S(1)}, u32[]{:S(2)}, u32[]{:S(2)}) %collective-permute-start.18) | collective-permute-done | bytes 131104 | tf_op jit(solution)/shard_map/ppermute | solution.py:36
  77.9 2.8 %collective-permute-done.26.refs_2_ = bf16[256,256]{1,0:T(8,128)(2,1)S(1)} collective-permute-done((bf16[256,256]{1,0:T(8,128)(2,1)S(1)}, bf16[256,256]{1,0:T(8,128)(2,1)S(1)}, u32[]{:S(2)}, u32[]{:S(2)}) %collective-permute-start.26) | collective-permute-done | bytes 131104 | tf_op jit(solution)/shard_map/ppermute | solution.py:36
  80.7 0.5 collective-permute-start.33
  81.2 1.8 %collective-permute-done.34.refs_2_ = bf16[256,256]{1,0:T(8,128)(2,1)S(1)} collective-permute-done((bf16[256,256]{1,0:T(8,128)(2,1)S(1)}, bf16[256,256]{1,0:T(8,128)(2,1)S(1)}, u32[]{:S(2)}, u32[]{:S(2)}) %collective-permute-start.34) | collective-permute-done | bytes 131104 | tf_op jit(solution)/shard_map/ppermute | solution.py:36
  83.0 0.5 collective-permute-start.10
  83.5 0.1 collective-permute-start.12
  83.6 1.0 shard_map.160
  84.6 0.3 collective-permute-start.20
  84.9 1.0 shard_map.162
  86.0 1.7 %collective-permute-start.28 = (bf16[256,512]{1,0:T(8,128)(2,1)S(1)}, bf16[256,512]{1,0:T(8,128)(2,1)S(1)}, u32[]{:S(2)}, u32[]{:S(2)}) collective-permute-start(bf16[256,512]{1,0:T(8,128)(2,1)S(1)} %shard_map.162), channel_id=1, source_target_pairs={{0,8},{4,12},{8,0},{12,4},{1,9},{5,13},{9,1},{13,5},{2,10},{6,14},... | collective-permute-start | bytes 786440 | tf_op jit(solution)/shard_map/ppermute | solution.py:36
  87.7 1.0 shard_map.164
  88.6 1.6 %collective-permute-start.36 = (bf16[256,512]{1,0:T(8,128)(2,1)S(1)}, bf16[256,512]{1,0:T(8,128)(2,1)S(1)}, u32[]{:S(2)}, u32[]{:S(2)}) collective-permute-start(bf16[256,512]{1,0:T(8,128)(2,1)S(1)} %shard_map.164), channel_id=1, source_target_pairs={{0,12},{4,8},{8,4},{12,0},{1,13},{5,9},{9,5},{13,1},{2,14},{6,10},... | collective-permute-start | bytes 786440 | tf_op jit(solution)/shard_map/ppermute | solution.py:36
  90.3 0.7 copy-done.16
  91.0 0.0 copy-done.15
  91.0 1.3 %shard_map.158.base_ref = f32[256,512]{1,0:T(8,128)S(1)} custom-call(s32[2]{0:T(128)S(1)} %pad_add_fusion.place_ref, s32[2,256]{1,0:T(2,128)S(1)} %bitcast.33, f32[2,256]{1,0:T(2,128)S(1)} %bitcast.35, bf16[4,256,512]{2,1,0:T(8,128)(2,1)S(1)} %bitcast.15, bf16[4,256,512]{2,1,0:T(8,128)(2,1)S(1)} %bitcast.24, ...), custom_call_target="tpu_custom_call" | custom-call | tf_op jit(solution)/shard_map/pallas_call | solution.py:189
  92.2 2.2 %collective-permute-done.20.refs_0_ = bf16[256,512]{1,0:T(8,128)(2,1)S(1)} collective-permute-done((bf16[256,512]{1,0:T(8,128)(2,1)S(1)}, bf16[256,512]{1,0:T(8,128)(2,1)S(1)}, u32[]{:S(2)}, u32[]{:S(2)}) %collective-permute-start.20) | collective-permute-done | bytes 262176 | tf_op jit(solution)/shard_map/ppermute | solution.py:36
  94.4 11.2 %collective-permute-done.28.refs_1_ = bf16[256,512]{1,0:T(8,128)(2,1)S(1)} collective-permute-done((bf16[256,512]{1,0:T(8,128)(2,1)S(1)}, bf16[256,512]{1,0:T(8,128)(2,1)S(1)}, u32[]{:S(2)}, u32[]{:S(2)}) %collective-permute-start.28) | collective-permute-done | bytes 262176 | tf_op jit(solution)/shard_map/ppermute | solution.py:36
  105.6 6.8 %collective-permute-done.36.refs_2_ = bf16[256,512]{1,0:T(8,128)(2,1)S(1)} collective-permute-done((bf16[256,512]{1,0:T(8,128)(2,1)S(1)}, bf16[256,512]{1,0:T(8,128)(2,1)S(1)}, u32[]{:S(2)}, u32[]{:S(2)}) %collective-permute-start.36) | collective-permute-done | bytes 262176 | tf_op jit(solution)/shard_map/ppermute | solution.py:36
  112.5 1.7 %shard_map.165 = bf16[256,512]{1,0:T(8,128)(2,1)} custom-call(s32[2]{0:T(128)S(1)} %pad_add_fusion.place_ref, s32[2,256]{1,0:T(2,128)S(1)} %bitcast.34, f32[2,256]{1,0:T(2,128)S(1)} %bitcast.36, f32[256,512]{1,0:T(8,128)S(1)} %shard_map.158.base_ref, bf16[256,512]{1,0:T(8,128)(2,1)S(1)} %collective-permute-done.20.refs_0_, ...), custom_call_target="tpu_custom_call" | custom-call | tf_op jit(solution)/shard_map/pallas_call | solution.py:189
  (62 shorter events, 0.2 us)
Async XLA Ops:
  0.0 0.7 copy-start.18
  0.8 1.2 %copy-start.3 = (bf16[256,2048]{1,0:T(8,128)(2,1)S(1)}, bf16[256,2048]{1,0:T(8,128)(2,1)}, u32[]{:S(2)}) copy-start(bf16[256,2048]{1,0:T(8,128)(2,1)} %weight_ref.1) | copy-start | bytes 3145732
  2.0 0.8 copy-start.9
  2.8 0.8 copy-start.11
  3.7 6.8 %copy-start.10 = (bf16[256,128]{1,0:T(8,128)(2,1)S(1)}, bf16[256,128]{1,0:T(8,128)(2,1)}, u32[]{:S(2)}) copy-start(bf16[256,128]{1,0:T(8,128)(2,1)} %k_ref.3) | copy-start | bytes 196612
  3.7 6.8 %copy-start.12 = (bf16[256,128]{1,0:T(8,128)(2,1)S(1)}, bf16[256,128]{1,0:T(8,128)(2,1)}, u32[]{:S(2)}) copy-start(bf16[256,128]{1,0:T(8,128)(2,1)} %v_ref.3) | copy-start | bytes 196612
  3.7 22.7 %copy-start.4 = (bf16[256,2048]{1,0:T(8,128)(2,1)S(1)}, bf16[256,2048]{1,0:T(8,128)(2,1)}, u32[]{:S(2)}) copy-start(bf16[256,2048]{1,0:T(8,128)(2,1)} %weight_ref.1) | copy-start | bytes 3145732
  4.3 6.2 %collective-permute-start = (bf16[272,128]{1,0:T(8,128)(2,1)S(1)}, bf16[272,128]{1,0:T(8,128)(2,1)S(1)}, u32[]{:S(2)}, u32[]{:S(2)}) collective-permute-start(bf16[272,128]{1,0:T(8,128)(2,1)S(1)} %get-tuple-element.9), channel_id=1, source_target_pairs={{0,4},{4,8},{8,12},{1,5},{5,9},{9,13},{2,6},{6,10},{10,14},{3,7},{... | collective-permute-start | bytes 208904 | tf_op jit(solution)/shard_map/ppermute | solution.py:21
  7.8 17.2 %collective-permute-start.4 = (bf16[256,512]{1,0:T(8,128)(2,1)S(1)}, bf16[256,512]{1,0:T(8,128)(2,1)S(1)}, u32[]{:S(2)}, u32[]{:S(2)}) collective-permute-start(bf16[256,512]{1,0:T(8,128)(2,1)S(1)} %get-tuple-element.10), channel_id=1, source_target_pairs={{0,1},{1,0},{2,3},{3,2},{4,5},{5,4},{6,7},{7,6},{8,9},{9,8},{10,11... | collective-permute-start | bytes 786440 | tf_op jit(solution)/shard_map/ppermute | solution.py:36
  7.9 2.6 %copy-start.17 = (f32[4]{0:T(128)S(1)}, f32[4]{0:T(128)}, u32[]{:S(2)}) copy-start(f32[4]{0:T(128)} %sink_ref.1) | copy-start | bytes 52
  7.9 17.1 %collective-permute-start.5 = (bf16[256,512]{1,0:T(8,128)(2,1)S(1)}, bf16[256,512]{1,0:T(8,128)(2,1)S(1)}, u32[]{:S(2)}, u32[]{:S(2)}) collective-permute-start(bf16[256,512]{1,0:T(8,128)(2,1)S(1)} %get-tuple-element.11), channel_id=1, source_target_pairs={{0,2},{1,3},{2,0},{3,1},{4,6},{5,7},{6,4},{7,5},{8,10},{9,11},{10,... | collective-permute-start | bytes 786440 | tf_op jit(solution)/shard_map/ppermute | solution.py:36
  8.5 16.6 %collective-permute-start.6 = (bf16[256,512]{1,0:T(8,128)(2,1)S(1)}, bf16[256,512]{1,0:T(8,128)(2,1)S(1)}, u32[]{:S(2)}, u32[]{:S(2)}) collective-permute-start(bf16[256,512]{1,0:T(8,128)(2,1)S(1)} %get-tuple-element.12), channel_id=1, source_target_pairs={{0,3},{1,2},{2,1},{3,0},{4,7},{5,6},{6,5},{7,4},{8,11},{9,10},{10,... | collective-permute-start | bytes 786440 | tf_op jit(solution)/shard_map/ppermute | solution.py:36
  10.5 0.9 copy-start.14
  13.4 49.1 %copy-start.1 = (bf16[1,2048,256]{2,1,0:T(8,128)(2,1)S(1)}, bf16[1,2048,256]{2,1,0:T(8,128)(2,1)}, u32[]{:S(2)}) copy-start(bf16[1,2048,256]{2,1,0:T(8,128)(2,1)} %param.26) | copy-start | bytes 3145732
  13.4 49.1 %copy-start.2 = (bf16[1,2048,256]{2,1,0:T(8,128)(2,1)S(1)}, bf16[1,2048,256]{2,1,0:T(8,128)(2,1)}, u32[]{:S(2)}) copy-start(bf16[1,2048,256]{2,1,0:T(8,128)(2,1)} %param.27) | copy-start | bytes 3145732
  13.4 11.6 %collective-permute-start.2 = (bf16[256,256]{1,0:T(8,128)(2,1)S(1)}, bf16[256,256]{1,0:T(8,128)(2,1)S(1)}, u32[]{:S(2)}, u32[]{:S(2)}) collective-permute-start(bf16[256,256]{1,0:T(8,128)(2,1)S(1)} %shard_map.155.refs_0_), channel_id=1, source_target_pairs={{0,2},{1,3},{2,0},{3,1},{4,6},{5,7},{6,4},{7,5},{8,10},{9,11},{10,... | collective-permute-start | bytes 393224 | tf_op jit(solution)/shard_map/ppermute | solution.py:36
  14.0 11.0 %collective-permute-start.1 = (bf16[256,256]{1,0:T(8,128)(2,1)S(1)}, bf16[256,256]{1,0:T(8,128)(2,1)S(1)}, u32[]{:S(2)}, u32[]{:S(2)}) collective-permute-start(bf16[256,256]{1,0:T(8,128)(2,1)S(1)} %shard_map.155.refs_0_), channel_id=1, source_target_pairs={{0,1},{1,0},{2,3},{3,2},{4,5},{5,4},{6,7},{7,6},{8,9},{9,8},{10,11... | collective-permute-start | bytes 393224 | tf_op jit(solution)/shard_map/ppermute | solution.py:36
  25.0 1.3 %collective-permute-start.3 = (bf16[256,256]{1,0:T(8,128)(2,1)S(1)}, bf16[256,256]{1,0:T(8,128)(2,1)S(1)}, u32[]{:S(2)}, u32[]{:S(2)}) collective-permute-start(bf16[256,256]{1,0:T(8,128)(2,1)S(1)} %collective-permute-done.2.refs_2_), channel_id=1, source_target_pairs={{0,1},{1,0},{2,3},{3,2},{4,5},{5,4},{6,7},{7,6},{8,9},{9,8},{10,11... | collective-permute-start | bytes 393224 | tf_op jit(solution)/shard_map/ppermute | solution.py:36
  26.3 1.2 %copy-start.6 = (bf16[256,2048]{1,0:T(8,128)(2,1)S(1)}, bf16[256,2048]{1,0:T(8,128)(2,1)}, u32[]{:S(2)}) copy-start(bf16[256,2048]{1,0:T(8,128)(2,1)} %residual_ref.1) | copy-start | bytes 3145732
  27.6 34.9 %copy-start.7 = (bf16[2048,256]{1,0:T(8,128)(2,1)S(1)}, bf16[2048,256]{1,0:T(8,128)(2,1)}, u32[]{:S(2)}) copy-start(bf16[2048,256]{1,0:T(8,128)(2,1)} %param.29) | copy-start | bytes 3145732
  28.6 33.9 %copy-start.13 = (f32[2048]{0:T(1024)S(1)}, f32[2048]{0:T(1024)}, u32[]{:S(2)}) copy-start(f32[2048]{0:T(1024)} %param.25) | copy-start | bytes 24580
  28.6 12.0 %collective-permute-start.21 = (bf16[256,512]{1,0:T(8,128)(2,1)S(1)}, bf16[256,512]{1,0:T(8,128)(2,1)S(1)}, u32[]{:S(2)}, u32[]{:S(2)}) collective-permute-start(bf16[256,512]{1,0:T(8,128)(2,1)S(1)} %shard_map.156.refs_0_.updated_ref), channel_id=1, source_target_pairs={{0,8},{4,12},{8,0},{12,4},{1,9},{5,13},{9,1},{13,5},{2,10},{6,14},... | collective-permute-start | bytes 786440 | tf_op jit(solution)/shard_map/ppermute | solution.py:36
  29.0 15.0 %collective-permute-start.13 = (bf16[256,512]{1,0:T(8,128)(2,1)S(1)}, bf16[256,512]{1,0:T(8,128)(2,1)S(1)}, u32[]{:S(2)}, u32[]{:S(2)}) collective-permute-start(bf16[256,512]{1,0:T(8,128)(2,1)S(1)} %shard_map.156.refs_0_.updated_ref), channel_id=1, source_target_pairs={{0,4},{4,0},{8,12},{12,8},{1,5},{5,1},{9,13},{13,9},{2,6},{6,2},{1... | collective-permute-start | bytes 786440 | tf_op jit(solution)/shard_map/ppermute | solution.py:36
  31.7 12.9 %collective-permute-start.8 = (bf16[256,512]{1,0:T(8,128)(2,1)S(1)}, bf16[256,512]{1,0:T(8,128)(2,1)S(1)}, u32[]{:S(2)}, u32[]{:S(2)}) collective-permute-start(bf16[256,512]{1,0:T(8,128)(2,1)S(1)} %shard_map.156.refs_0_.updated_ref), channel_id=1, source_target_pairs={{0,2},{1,3},{2,0},{3,1},{4,6},{5,7},{6,4},{7,5},{8,10},{9,11},{10,... | collective-permute-start | bytes 786440 | tf_op jit(solution)/shard_map/ppermute | solution.py:36
  32.2 13.9 %collective-permute-start.7 = (bf16[256,512]{1,0:T(8,128)(2,1)S(1)}, bf16[256,512]{1,0:T(8,128)(2,1)S(1)}, u32[]{:S(2)}, u32[]{:S(2)}) collective-permute-start(bf16[256,512]{1,0:T(8,128)(2,1)S(1)} %shard_map.156.refs_0_.updated_ref), channel_id=1, source_target_pairs={{0,1},{1,0},{2,3},{3,2},{4,5},{5,4},{6,7},{7,6},{8,9},{9,8},{10,11... | collective-permute-start | bytes 786440 | tf_op jit(solution)/shard_map/ppermute | solution.py:36
  40.5 9.2 %collective-permute-start.29 = (bf16[256,512]{1,0:T(8,128)(2,1)S(1)}, bf16[256,512]{1,0:T(8,128)(2,1)S(1)}, u32[]{:S(2)}, u32[]{:S(2)}) collective-permute-start(bf16[256,512]{1,0:T(8,128)(2,1)S(1)} %collective-permute-done.21.refs_0_), channel_id=1, source_target_pairs={{0,4},{4,0},{8,12},{12,8},{1,5},{5,1},{9,13},{13,9},{2,6},{6,2},{1... | collective-permute-start | bytes 786440 | tf_op jit(solution)/shard_map/ppermute | solution.py:36
  44.1 9.2 %collective-permute-start.15 = (bf16[256,512]{1,0:T(8,128)(2,1)S(1)}, bf16[256,512]{1,0:T(8,128)(2,1)S(1)}, u32[]{:S(2)}, u32[]{:S(2)}) collective-permute-start(bf16[256,512]{1,0:T(8,128)(2,1)S(1)} %collective-permute-done.13.refs_0_), channel_id=1, source_target_pairs={{0,2},{1,3},{2,0},{3,1},{4,6},{5,7},{6,4},{7,5},{8,10},{9,11},{10,... | collective-permute-start | bytes 786440 | tf_op jit(solution)/shard_map/ppermute | solution.py:36
  44.6 8.6 %collective-permute-start.9 = (bf16[256,512]{1,0:T(8,128)(2,1)S(1)}, bf16[256,512]{1,0:T(8,128)(2,1)S(1)}, u32[]{:S(2)}, u32[]{:S(2)}) collective-permute-start(bf16[256,512]{1,0:T(8,128)(2,1)S(1)} %collective-permute-done.8.refs_2_), channel_id=1, source_target_pairs={{0,1},{1,0},{2,3},{3,2},{4,5},{5,4},{6,7},{7,6},{8,9},{9,8},{10,11... | collective-permute-start | bytes 786440 | tf_op jit(solution)/shard_map/ppermute | solution.py:36
  44.6 14.3 %collective-permute-start.23 = (bf16[256,512]{1,0:T(8,128)(2,1)S(1)}, bf16[256,512]{1,0:T(8,128)(2,1)S(1)}, u32[]{:S(2)}, u32[]{:S(2)}) collective-permute-start(bf16[256,512]{1,0:T(8,128)(2,1)S(1)} %collective-permute-done.21.refs_0_), channel_id=1, source_target_pairs={{0,2},{1,3},{2,0},{3,1},{4,6},{5,7},{6,4},{7,5},{8,10},{9,11},{10,... | collective-permute-start | bytes 786440 | tf_op jit(solution)/shard_map/ppermute | solution.py:36
  46.1 12.8 %collective-permute-start.14 = (bf16[256,512]{1,0:T(8,128)(2,1)S(1)}, bf16[256,512]{1,0:T(8,128)(2,1)S(1)}, u32[]{:S(2)}, u32[]{:S(2)}) collective-permute-start(bf16[256,512]{1,0:T(8,128)(2,1)S(1)} %collective-permute-done.13.refs_0_), channel_id=1, source_target_pairs={{0,1},{1,0},{2,3},{3,2},{4,5},{5,4},{6,7},{7,6},{8,9},{9,8},{10,11... | collective-permute-start | bytes 786440 | tf_op jit(solution)/shard_map/ppermute | solution.py:36
  49.8 12.7 %collective-permute-start.31 = (bf16[256,512]{1,0:T(8,128)(2,1)S(1)}, bf16[256,512]{1,0:T(8,128)(2,1)S(1)}, u32[]{:S(2)}, u32[]{:S(2)}) collective-permute-start(bf16[256,512]{1,0:T(8,128)(2,1)S(1)} %collective-permute-done.29.refs_0_), channel_id=1, source_target_pairs={{0,2},{1,3},{2,0},{3,1},{4,6},{5,7},{6,4},{7,5},{8,10},{9,11},{10,... | collective-permute-start | bytes 786440 | tf_op jit(solution)/shard_map/ppermute | solution.py:36
  53.2 12.6 %collective-permute-start.16 = (bf16[256,512]{1,0:T(8,128)(2,1)S(1)}, bf16[256,512]{1,0:T(8,128)(2,1)S(1)}, u32[]{:S(2)}, u32[]{:S(2)}) collective-permute-start(bf16[256,512]{1,0:T(8,128)(2,1)S(1)} %collective-permute-done.15.refs_2_), channel_id=1, source_target_pairs={{0,1},{1,0},{2,3},{3,2},{4,5},{5,4},{6,7},{7,6},{8,9},{9,8},{10,11... | collective-permute-start | bytes 786440 | tf_op jit(solution)/shard_map/ppermute | solution.py:36
  53.3 14.7 %collective-permute-start.22 = (bf16[256,512]{1,0:T(8,128)(2,1)S(1)}, bf16[256,512]{1,0:T(8,128)(2,1)S(1)}, u32[]{:S(2)}, u32[]{:S(2)}) collective-permute-start(bf16[256,512]{1,0:T(8,128)(2,1)S(1)} %collective-permute-done.21.refs_0_), channel_id=1, source_target_pairs={{0,1},{1,0},{2,3},{3,2},{4,5},{5,4},{6,7},{7,6},{8,9},{9,8},{10,11... | collective-permute-start | bytes 786440 | tf_op jit(solution)/shard_map/ppermute | solution.py:36
  58.9 10.6 %collective-permute-start.24 = (bf16[256,512]{1,0:T(8,128)(2,1)S(1)}, bf16[256,512]{1,0:T(8,128)(2,1)S(1)}, u32[]{:S(2)}, u32[]{:S(2)}) collective-permute-start(bf16[256,512]{1,0:T(8,128)(2,1)S(1)} %collective-permute-done.23.refs_2_), channel_id=1, source_target_pairs={{0,1},{1,0},{2,3},{3,2},{4,5},{5,4},{6,7},{7,6},{8,9},{9,8},{10,11... | collective-permute-start | bytes 786440 | tf_op jit(solution)/shard_map/ppermute | solution.py:36
  58.9 12.7 %collective-permute-start.30 = (bf16[256,512]{1,0:T(8,128)(2,1)S(1)}, bf16[256,512]{1,0:T(8,128)(2,1)S(1)}, u32[]{:S(2)}, u32[]{:S(2)}) collective-permute-start(bf16[256,512]{1,0:T(8,128)(2,1)S(1)} %collective-permute-done.29.refs_0_), channel_id=1, source_target_pairs={{0,1},{1,0},{2,3},{3,2},{4,5},{5,4},{6,7},{7,6},{8,9},{9,8},{10,11... | collective-permute-start | bytes 786440 | tf_op jit(solution)/shard_map/ppermute | solution.py:36
  62.5 9.1 %collective-permute-start.32 = (bf16[256,512]{1,0:T(8,128)(2,1)S(1)}, bf16[256,512]{1,0:T(8,128)(2,1)S(1)}, u32[]{:S(2)}, u32[]{:S(2)}) collective-permute-start(bf16[256,512]{1,0:T(8,128)(2,1)S(1)} %collective-permute-done.31.refs_2_), channel_id=1, source_target_pairs={{0,1},{1,0},{2,3},{3,2},{4,5},{5,4},{6,7},{7,6},{8,9},{9,8},{10,11... | collective-permute-start | bytes 786440 | tf_op jit(solution)/shard_map/ppermute | solution.py:36
  62.5 1.2 %copy-start.8 = (bf16[2048,256]{1,0:T(8,128)(2,1)S(1)}, bf16[2048,256]{1,0:T(8,128)(2,1)}, u32[]{:S(2)}) copy-start(bf16[2048,256]{1,0:T(8,128)(2,1)} %param.30) | copy-start | bytes 3145732
  65.8 9.2 %collective-permute-start.11 = (bf16[256,512]{1,0:T(8,128)(2,1)S(1)}, bf16[256,512]{1,0:T(8,128)(2,1)S(1)}, u32[]{:S(2)}, u32[]{:S(2)}) collective-permute-start(bf16[256,512]{1,0:T(8,128)(2,1)S(1)} %shard_map.157.refs_0_), channel_id=1, source_target_pairs={{0,2},{1,3},{2,0},{3,1},{4,6},{5,7},{6,4},{7,5},{8,10},{9,11},{10,... | collective-permute-start | bytes 786440 | tf_op jit(solution)/shard_map/ppermute | solution.py:36
  67.9 9.9 %collective-permute-start.18 = (bf16[256,256]{1,0:T(8,128)(2,1)S(1)}, bf16[256,256]{1,0:T(8,128)(2,1)S(1)}, u32[]{:S(2)}, u32[]{:S(2)}) collective-permute-start(bf16[256,256]{1,0:T(8,128)(2,1)S(1)} %shard_map.159.refs_0_), channel_id=1, source_target_pairs={{0,2},{1,3},{2,0},{3,1},{4,6},{5,7},{6,4},{7,5},{8,10},{9,11},{10,... | collective-permute-start | bytes 393224 | tf_op jit(solution)/shard_map/ppermute | solution.py:36
  71.0 12.6 %copy-start = (bf16[1,1024,512]{2,1,0:T(8,128)(2,1)S(1)}, bf16[1,1024,512]{2,1,0:T(8,128)(2,1)}, u32[]{:S(2)}) copy-start(bf16[1,1024,512]{2,1,0:T(8,128)(2,1)} %param.28) | copy-start | bytes 3145732
  71.0 9.7 %collective-permute-start.26 = (bf16[256,256]{1,0:T(8,128)(2,1)S(1)}, bf16[256,256]{1,0:T(8,128)(2,1)S(1)}, u32[]{:S(2)}, u32[]{:S(2)}) collective-permute-start(bf16[256,256]{1,0:T(8,128)(2,1)S(1)} %shard_map.161.refs_0_), channel_id=1, source_target_pairs={{0,2},{1,3},{2,0},{3,1},{4,6},{5,7},{6,4},{7,5},{8,10},{9,11},{10,... | collective-permute-start | bytes 393224 | tf_op jit(solution)/shard_map/ppermute | solution.py:36
  71.6 9.1 %collective-permute-start.17 = (bf16[256,256]{1,0:T(8,128)(2,1)S(1)}, bf16[256,256]{1,0:T(8,128)(2,1)S(1)}, u32[]{:S(2)}, u32[]{:S(2)}) collective-permute-start(bf16[256,256]{1,0:T(8,128)(2,1)S(1)} %shard_map.159.refs_0_), channel_id=1, source_target_pairs={{0,1},{1,0},{2,3},{3,2},{4,5},{5,4},{6,7},{7,6},{8,9},{9,8},{10,11... | collective-permute-start | bytes 393224 | tf_op jit(solution)/shard_map/ppermute | solution.py:36
  73.1 9.9 %collective-permute-start.34 = (bf16[256,256]{1,0:T(8,128)(2,1)S(1)}, bf16[256,256]{1,0:T(8,128)(2,1)S(1)}, u32[]{:S(2)}, u32[]{:S(2)}) collective-permute-start(bf16[256,256]{1,0:T(8,128)(2,1)S(1)} %shard_map.163.refs_0_), channel_id=1, source_target_pairs={{0,2},{1,3},{2,0},{3,1},{4,6},{5,7},{6,4},{7,5},{8,10},{9,11},{10,... | collective-permute-start | bytes 393224 | tf_op jit(solution)/shard_map/ppermute | solution.py:36
  75.1 8.0 %collective-permute-start.25 = (bf16[256,256]{1,0:T(8,128)(2,1)S(1)}, bf16[256,256]{1,0:T(8,128)(2,1)S(1)}, u32[]{:S(2)}, u32[]{:S(2)}) collective-permute-start(bf16[256,256]{1,0:T(8,128)(2,1)S(1)} %shard_map.161.refs_0_), channel_id=1, source_target_pairs={{0,1},{1,0},{2,3},{3,2},{4,5},{5,4},{6,7},{7,6},{8,9},{9,8},{10,11... | collective-permute-start | bytes 393224 | tf_op jit(solution)/shard_map/ppermute | solution.py:36
  77.9 5.7 %collective-permute-start.19 = (bf16[256,256]{1,0:T(8,128)(2,1)S(1)}, bf16[256,256]{1,0:T(8,128)(2,1)S(1)}, u32[]{:S(2)}, u32[]{:S(2)}) collective-permute-start(bf16[256,256]{1,0:T(8,128)(2,1)S(1)} %collective-permute-done.18.refs_2_), channel_id=1, source_target_pairs={{0,1},{1,0},{2,3},{3,2},{4,5},{5,4},{6,7},{7,6},{8,9},{9,8},{10,11... | collective-permute-start | bytes 393224 | tf_op jit(solution)/shard_map/ppermute | solution.py:36
  80.7 3.9 %collective-permute-start.27 = (bf16[256,256]{1,0:T(8,128)(2,1)S(1)}, bf16[256,256]{1,0:T(8,128)(2,1)S(1)}, u32[]{:S(2)}, u32[]{:S(2)}) collective-permute-start(bf16[256,256]{1,0:T(8,128)(2,1)S(1)} %collective-permute-done.26.refs_2_), channel_id=1, source_target_pairs={{0,1},{1,0},{2,3},{3,2},{4,5},{5,4},{6,7},{7,6},{8,9},{9,8},{10,11... | collective-permute-start | bytes 393224 | tf_op jit(solution)/shard_map/ppermute | solution.py:36
  80.7 5.3 %collective-permute-start.33 = (bf16[256,256]{1,0:T(8,128)(2,1)S(1)}, bf16[256,256]{1,0:T(8,128)(2,1)S(1)}, u32[]{:S(2)}, u32[]{:S(2)}) collective-permute-start(bf16[256,256]{1,0:T(8,128)(2,1)S(1)} %shard_map.163.refs_0_), channel_id=1, source_target_pairs={{0,1},{1,0},{2,3},{3,2},{4,5},{5,4},{6,7},{7,6},{8,9},{9,8},{10,11... | collective-permute-start | bytes 393224 | tf_op jit(solution)/shard_map/ppermute | solution.py:36
  83.0 4.7 %collective-permute-start.35 = (bf16[256,256]{1,0:T(8,128)(2,1)S(1)}, bf16[256,256]{1,0:T(8,128)(2,1)S(1)}, u32[]{:S(2)}, u32[]{:S(2)}) collective-permute-start(bf16[256,256]{1,0:T(8,128)(2,1)S(1)} %collective-permute-done.34.refs_2_), channel_id=1, source_target_pairs={{0,1},{1,0},{2,3},{3,2},{4,5},{5,4},{6,7},{7,6},{8,9},{9,8},{10,11... | collective-permute-start | bytes 393224 | tf_op jit(solution)/shard_map/ppermute | solution.py:36
  83.0 7.3 %collective-permute-start.10 = (bf16[256,512]{1,0:T(8,128)(2,1)S(1)}, bf16[256,512]{1,0:T(8,128)(2,1)S(1)}, u32[]{:S(2)}, u32[]{:S(2)}) collective-permute-start(bf16[256,512]{1,0:T(8,128)(2,1)S(1)} %shard_map.157.refs_0_), channel_id=1, source_target_pairs={{0,1},{1,0},{2,3},{3,2},{4,5},{5,4},{6,7},{7,6},{8,9},{9,8},{10,11... | collective-permute-start | bytes 786440 | tf_op jit(solution)/shard_map/ppermute | solution.py:36
  83.5 6.7 %collective-permute-start.12 = (bf16[256,512]{1,0:T(8,128)(2,1)S(1)}, bf16[256,512]{1,0:T(8,128)(2,1)S(1)}, u32[]{:S(2)}, u32[]{:S(2)}) collective-permute-start(bf16[256,512]{1,0:T(8,128)(2,1)S(1)} %collective-permute-done.11.refs_2_), channel_id=1, source_target_pairs={{0,1},{1,0},{2,3},{3,2},{4,5},{5,4},{6,7},{7,6},{8,9},{9,8},{10,11... | collective-permute-start | bytes 786440 | tf_op jit(solution)/shard_map/ppermute | solution.py:36
  84.6 9.8 %collective-permute-start.20 = (bf16[256,512]{1,0:T(8,128)(2,1)S(1)}, bf16[256,512]{1,0:T(8,128)(2,1)S(1)}, u32[]{:S(2)}, u32[]{:S(2)}) collective-permute-start(bf16[256,512]{1,0:T(8,128)(2,1)S(1)} %shard_map.160), channel_id=1, source_target_pairs={{0,4},{4,0},{8,12},{12,8},{1,5},{5,1},{9,13},{13,9},{2,6},{6,2},{1... | collective-permute-start | bytes 786440 | tf_op jit(solution)/shard_map/ppermute | solution.py:36
  85.9 4.4 %copy-start.5 = (bf16[1024,512]{1,0:T(8,128)(2,1)S(1)}, bf16[1024,512]{1,0:T(8,128)(2,1)}, u32[]{:S(2)}) copy-start(bf16[1024,512]{1,0:T(8,128)(2,1)} %param.31) | copy-start | bytes 3145732
  86.0 19.7 %collective-permute-start.28 = (bf16[256,512]{1,0:T(8,128)(2,1)S(1)}, bf16[256,512]{1,0:T(8,128)(2,1)S(1)}, u32[]{:S(2)}, u32[]{:S(2)}) collective-permute-start(bf16[256,512]{1,0:T(8,128)(2,1)S(1)} %shard_map.162), channel_id=1, source_target_pairs={{0,8},{4,12},{8,0},{12,4},{1,9},{5,13},{9,1},{13,5},{2,10},{6,14},... | collective-permute-start | bytes 786440 | tf_op jit(solution)/shard_map/ppermute | solution.py:36
  88.6 23.8 %collective-permute-start.36 = (bf16[256,512]{1,0:T(8,128)(2,1)S(1)}, bf16[256,512]{1,0:T(8,128)(2,1)S(1)}, u32[]{:S(2)}, u32[]{:S(2)}) collective-permute-start(bf16[256,512]{1,0:T(8,128)(2,1)S(1)} %shard_map.164), channel_id=1, source_target_pairs={{0,12},{4,8},{8,4},{12,0},{1,13},{5,9},{9,5},{13,1},{2,14},{6,10},... | collective-permute-start | bytes 786440 | tf_op jit(solution)/shard_map/ppermute | solution.py:36
  90.3 0.7 copy-start.16
  90.3 0.7 copy-start.15
where the time goes:
time: 115 us; the launch traced here: 114 us
  waiting for transfers between devices  64.1 us (56%)
  starting transfers between devices  26.1 us (23%)
  Pallas kernels  15.9 us (14%)
  local copies, waits for them, and re-layouts  7.66 us (7%)
    ppermute x36, waiting for transfers between devices, swapped(): lax.ppermute(value, axis, [(source, source ^ bit) for source in range(cou...  63.3 us
    ppermute x36, starting transfers between devices, swapped(): lax.ppermute(value, axis, [(source, source ^ bit) for source in range(cou...  22.6 us
    pallas_call x12, Pallas kernels, call(): pl.pallas_call(kernel, out_shape=out, in_specs=specs, out_specs=[vmem] *...  15.9 us
    unnamed x38, local copies, waits for them, and re-layouts  7.66 us
    ppermute x1, starting transfers between devices, passed_along(): lax.ppermute(value, axis, [(source, source + steps) for source in range(l...  3.48 us
  transfers between devices with their start and end apart: 37, of which 15 were waited for; matrix products, arithmetic and copies ran while one was open for 0% of the time, Pallas kernels for 11%

commit v1 on v0

--- a/solution.py
+++ b/solution.py
@@ -36,14 +36,16 @@
     return lax.ppermute(value, axis, [(source, source ^ bit) for source in range(count)])
 
 
-def gathered(value):
+def gathered(value, far=None):
     pieces = {0: value}
     bit = lax.axis_size("tp") // 2
     while bit:
         more = {}
         for known, held in pieces.items():
-            more[known ^ bit] = swapped(held, "tp", bit)
+            j = known ^ bit
+            more[j] = swapped(held, "tp", bit) if far is None or known else far
         pieces.update(more)
+        far = None
         bit //= 2
     return [pieces[j] for j in range(len(pieces))]
 
@@ -52,27 +54,51 @@
     return jnp.dot(left, right, preferred_element_type=jnp.float32)
 
 
-def columns(ref, spot):
-    width = ref.shape[1] // lax.axis_size("tp")
-    return ref[:, pl.ds(pl.multiple_of(spot * width, width), width)]
+def own_columns(ref, spot, width):
+    return ref.at[:, pl.ds(pl.multiple_of(spot * width, width), width)]
+
+
+def copy_all(sources, targets, sems):
+    copies = [
+        pltpu.make_async_copy(source, target, sems.at[n])
+        for n, (source, target) in enumerate(zip(sources, targets, strict=True))
+    ]
+    for copy in copies:
+        copy.start()
+    for copy in copies:
+        copy.wait()
 
 
 def column(row):
     return jnp.transpose(jnp.broadcast_to(row, (8, row.shape[1])))[:, :1]
 
 
-def prologue_kernel(place_ref, marks_ref, k_ref, v_ref, out_ref, packed_ref, *part_refs):
-    span, rows = WINDOW, k_ref.shape[0]
+def prologue_kernel(marks_hbm, k_hbm, v_hbm, weight_hbm, packed_ref, row_ref, *refs):
+    part_refs, sems = refs[:-1], refs[-1]
+    span, rows = WINDOW, k_hbm.shape[0]
+    place = lax.axis_index("tp")
     tail = slice(rows - span, rows)
-    packed_ref[:span, :] = k_ref[tail, :]
-    packed_ref[span : 2 * span, :] = v_ref[tail, :]
-    marks = jnp.broadcast_to(marks_ref[:, tail], (packed_ref.shape[0] - 2 * span, span))
+    parts = [own_columns(weight_hbm, place ^ j, part.shape[1]) for j, part in enumerate(part_refs, 1)]
+    copy_all(
+        [marks_hbm, k_hbm.at[tail], v_hbm.at[tail], *parts],
+        [row_ref, packed_ref.at[:span], packed_ref.at[span : 2 * span], *part_refs],
+        sems,
+    )
+    marks = jnp.bitwise_and(row_ref[:, tail], 255) + 1
+    marks = jnp.broadcast_to(marks.astype(jnp.float32), (packed_ref.shape[0] - 2 * span, span))
     packed_ref[2 * span :, :] = marks.astype(jnp.bfloat16)
-    for j, part_ref in enumerate(part_refs, 1):
-        part_ref[...] = columns(out_ref, place_ref[0] ^ j)
-
-
-def attend_kernel(sink_ref, row_ref, q_ref, k_ref, v_ref, halo_ref, out_ref):
+
+
+def fetch_kernel(count, sliced, *refs):
+    sources, targets, sems = refs[:count], refs[count:-1], refs[-1]
+    place = lax.axis_index("tp")
+    cut = [own_columns(source, place, target.shape[1]) for source, target in zip(sources[:sliced], targets)]
+    copy_all([*cut, *sources[sliced:]], targets, sems)
+
+
+def attend_kernel(sink_hbm, row_ref, q_ref, k_ref, v_ref, halo_ref, out_ref, sink_ref, sem):
+    copy = pltpu.make_async_copy(sink_hbm, sink_ref, sem)
+    copy.start()
     span = WINDOW
     rows = q_ref.shape[0]
     kv_local = k_ref.shape[1] // HEAD_DIM
@@ -80,12 +106,13 @@
     halo = halo_ref[...]
     keys = jnp.concatenate([halo[:span], k_ref[...]], axis=0)
     values = jnp.concatenate([halo[span : 2 * span], v_ref[...]], axis=0)
-    own = row_ref[...]
+    own = (jnp.bitwise_and(row_ref[...], 255) + 1).astype(jnp.float32)
     marks = jnp.concatenate([halo[2 * span : 2 * span + 1].astype(jnp.float32), own], axis=1)
     down_marks = column(own)
     place = lax.broadcasted_iota(jnp.int32, (span, 2 * span), 0)
     offsets = place + span - lax.broadcasted_iota(jnp.int32, (span, 2 * span), 1)
     near = (offsets >= 0) & (offsets < span)
+    copy.wait()
     for block in range(rows // span):
         low = block * span
         allowed = near & (down_marks[low : low + span] == marks[:, low : low + 2 * span])
@@ -110,19 +137,16 @@
         out_ref[low : low + span, :] = jnp.concatenate(outs, axis=1)
 
 
-def update_kernel(count, place_ref, residual_ref, weight_ref, *refs):
-    acts, parts, out_ref = refs[:count], refs[count:-1], refs[-1]
-    place = place_ref[0]
-    total = columns(residual_ref, place).astype(jnp.float32)
-    total = total + dot32(acts[0][...], columns(weight_ref, place))
-    for act, part in zip(acts[1:], parts, strict=True):
-        total = total + dot32(act[...], part[...])
-    out_ref[...] = total.astype(jnp.bfloat16)
-
-
-def hidden_kernel(count, pairs, place_ref, gain_ref, *refs):
+def update_kernel(count, residual_ref, *refs):
+    total = residual_ref[...].astype(jnp.float32)
+    for j in range(count):
+        total = total + dot32(refs[j][...], refs[count + j][...])
+    refs[-1][...] = total.astype(jnp.bfloat16)
+
+
+def hidden_kernel(count, pairs, gain_ref, *refs):
     pieces, weights, out_ref = refs[:count], refs[count:-1], refs[-1]
-    place = place_ref[0]
+    place = lax.axis_index("tp")
     width = sum(piece.shape[1] for piece in pieces)
     hidden = weights[0].shape[2]
     squares = 0.0
@@ -143,16 +167,16 @@
         out_ref[:, n * hidden : (n + 1) * hidden] = act.astype(jnp.bfloat16)
 
 
-def down_kernel(count, place_ref, down_ref, *refs):
-    place = place_ref[0]
+def down_kernel(count, down_ref, *refs):
+    place = lax.axis_index("tp")
     total = dot32(refs[0][...], down_ref[place])
     for j in range(1, count):
         total = total + dot32(refs[j][...], down_ref[place ^ j])
     refs[-1][...] = total.astype(jnp.bfloat16)
 
 
-def weights_of(spot, routes_ref, weight_ref, steps):
-    routes, weight = routes_ref[...], weight_ref[...]
+def weights_of(routes_ref, weight_ref, steps):
+    routes, weight, spot = routes_ref[...], weight_ref[...], lax.axis_index("sp")
     rows = []
     for k in range(steps):
         named = jnp.where(routes == (spot ^ k), weight, 0.0)
@@ -161,8 +185,8 @@
     return jnp.transpose(jnp.concatenate(rows, axis=0))
 
 
-def own_kernel(count, place_ref, routes_ref, weight_ref, down_ref, shared_ref, updated_ref, *refs):
-    place = place_ref[0]
+def own_kernel(count, routes_ref, weight_ref, down_ref, shared_ref, updated_ref, *refs):
+    place = lax.axis_index("tp")
     hidden = down_ref.shape[1]
     for j in range(count):
         terms = [
@@ -170,29 +194,51 @@
             dot32(refs[j][:, hidden:], shared_ref[place ^ j]),
         ]
         sums = terms if j == 0 else [old + term for old, term in zip(sums, terms, strict=True)]
-    weight = weights_of(place_ref[1], routes_ref, weight_ref, 1)[:, :1]
+    weight = weights_of(routes_ref, weight_ref, 1)[:, :1]
     routed = sums[0].astype(jnp.bfloat16).astype(jnp.float32)
     refs[-1][...] = updated_ref[...].astype(jnp.float32) + sums[1] + routed * weight
 
 
-def mix_kernel(count, place_ref, routes_ref, weight_ref, base_ref, *refs):
-    weights = weights_of(place_ref[1], routes_ref, weight_ref, count + 1)
+def mix_kernel(count, routes_ref, weight_ref, base_ref, *refs):
+    weights = weights_of(routes_ref, weight_ref, count + 1)
     total = base_ref[...]
     for k in range(count):
         total = total + refs[k][...].astype(jnp.float32) * weights[:, k + 1 : k + 2]
     refs[-1][...] = total.astype(jnp.bfloat16)
 
 
-def call(kernel, out, args, scalars=1):
-    specs = [pl.BlockSpec(memory_space=pltpu.SMEM if n < scalars else pltpu.VMEM) for n in range(len(args))]
+def call(kernel, out, args, scalars=None):
     vmem = pl.BlockSpec(memory_space=pltpu.VMEM)
+    specs, scratch = [vmem] * len(args), []
+    if scalars is not None:
+        args = [pltpu.with_memory_space_constraint(scalars, pltpu.HBM), *args]
+        specs = [pl.BlockSpec(memory_space=pltpu.HBM), *specs]
+        scratch = [pltpu.SMEM(scalars.shape, scalars.dtype), pltpu.SemaphoreType.DMA]
     return pl.pallas_call(
         kernel,
         out_shape=out,
         in_specs=specs,
-        out_specs=[vmem] * len(out) if isinstance(out, list) else vmem,
+        out_specs=vmem,
+        scratch_shapes=scratch,
         compiler_params=pltpu.CompilerParams(vmem_limit_bytes=KERNEL_VMEM),
     )(*args)
+
+
+def copier(kernel, outs, args, extra=0):
+    args = [pltpu.with_memory_space_constraint(arg, pltpu.HBM) for arg in args]
+    return pl.pallas_call(
+        kernel,
+        out_shape=[pltpu.VMEM(shape, dtype) for shape, dtype in outs],
+        in_specs=[pl.BlockSpec(memory_space=pltpu.HBM)] * len(args),
+        out_specs=[pl.BlockSpec(memory_space=pltpu.VMEM)] * len(outs),
+        scratch_shapes=[pltpu.SemaphoreType.DMA((len(outs) + extra,))],
+        compiler_params=pltpu.CompilerParams(vmem_limit_bytes=KERNEL_VMEM),
+    )(*args)
+
+
+def fetched(args, width=0, sliced=0):
+    outs = [(arg.shape[:1] + (width,) if n < sliced else arg.shape, arg.dtype) for n, arg in enumerate(args)]
+    return copier(functools.partial(fetch_kernel, len(args), sliced), outs, args)
 
 
 def dense_shards(*args):
@@ -219,31 +265,26 @@
 ):
     rows_here, model_width = residual.shape
     tp_count, sp_count = lax.axis_size("tp"), lax.axis_size("sp")
-    tp_index = lax.axis_index("tp").astype(jnp.int32)
-    sp_index = lax.axis_index("sp").astype(jnp.int32)
-    place = jnp.stack([tp_index, sp_index])
     span = WINDOW
     col_width = model_width // tp_count
     heads_width = out_weight.shape[0]
     bf16, f32 = jnp.bfloat16, jnp.float32
     shape = jax.ShapeDtypeStruct
-
-    own_marks = (segments % 256 + 1).astype(f32)[None, :]
-    packed, *parts = call(
+    segments = segments[None, :]
+
+    packed, _, *parts = copier(
         prologue_kernel,
-        [shape((2 * span + 16, span), bf16)] + [shape((heads_width, col_width), bf16)] * (tp_count - 1),
-        [place, own_marks, keys, values, out_weight],
+        [((2 * span + 16, span), bf16), (segments.shape, segments.dtype)]
+        + [((heads_width, col_width), bf16)] * (tp_count - 1),
+        [segments, keys, values, out_weight],
+        1,
     )
     halo = passed_along(packed, "sp", 1)
     parts = [swapped(part, "tp", j) for j, part in enumerate(parts, 1)]
-    attended = call(
-        attend_kernel, shape(queries.shape, bf16), [sinks, own_marks, queries, keys, values, halo]
-    )
-    own = call(
-        functools.partial(update_kernel, tp_count),
-        shape((rows_here, col_width), bf16),
-        [place, residual, out_weight, *gathered(attended), *parts],
-    )
+    residual_cols, own_part, marks, own_queries, own_keys, own_values = fetched(
+        [residual, out_weight, segments, queries, keys, values], col_width, 2
+    )
+    attended = call(attend_kernel, shape(queries.shape, bf16), [marks, own_queries, own_keys, own_values, halo], sinks)
 
     gain = norm_gain.reshape(tp_count, 1, col_width)
     gate, up, common_gate, common_up = [
@@ -251,39 +292,44 @@
     ]
     hidden = gate.shape[2]
     down, common_down = [weight.reshape(tp_count, hidden, col_width) for weight in (expert_down, shared_down)]
-    routes, route_weight = routes.T, route_weight.T
+    gain, gate, up, common_gate, common_up, down, common_down, routes, route_weight = fetched(
+        [gain, gate, up, common_gate, common_up, down, common_down, routes.T, route_weight.T]
+    )
+    own = call(
+        functools.partial(update_kernel, tp_count),
+        shape((rows_here, col_width), bf16),
+        [residual_cols, *gathered(attended), own_part, *parts],
+    )
     cols = (rows_here, col_width)
 
-    blocks = [own] + [swapped(own, "sp", k) for k in range(1, sp_count - 1)]
-    blocks.append(swapped(blocks[(sp_count - 1) ^ 1], "sp", 1))
+    last, half = sp_count - 1, tp_count // 2
+    blocks = [gathered(own)]
+    for k in range(1, last):
+        blocks.append(gathered(swapped(own, "sp", k)))
+    near, far = [swapped(blocks[last ^ 1][j], "sp", 1) for j in (0, half)]
+    blocks.append(gathered(near, far))
     returned = []
     base = None
     for k in range(sp_count):
-        pieces = gathered(blocks[k])
+        pieces = blocks[k]
         pairs = 2 if k == 0 else 1
         weights = [gate, up, common_gate, common_up][: 2 * pairs]
         act = call(
             functools.partial(hidden_kernel, tp_count, pairs),
             shape((rows_here, pairs * hidden), bf16),
-            [place, gain, *pieces, *weights],
+            [gain, *pieces, *weights],
         )
         acts = gathered(act)
         if k == 0:
             base = call(
                 functools.partial(own_kernel, tp_count),
                 shape(cols, f32),
-                [place, routes, route_weight, down, common_down, own, *acts],
+                [routes, route_weight, down, common_down, own, *acts],
             )
         else:
-            out = call(
-                functools.partial(down_kernel, tp_count), shape(cols, bf16), [place, down, *acts]
-            )
+            out = call(functools.partial(down_kernel, tp_count), shape(cols, bf16), [down, *acts])
             returned.append(swapped(out, "sp", k))
-    return call(
-        functools.partial(mix_kernel, sp_count - 1),
-        shape(cols, bf16),
-        [place, routes, route_weight, base, *returned],
-    )
+    return call(functools.partial(mix_kernel, sp_count - 1), shape(cols, bf16), [routes, route_weight, base, *returned])
 
 
 def shards(

time: 115 us -> 104 us (0.904)
  the two profiles are of different devices: /device:TPU:10 before, /device:TPU:9 now
where the time goes in v1:
time: 104 us
  waiting for transfers between devices  46.7 us (45%)
  starting transfers between devices  41.1 us (40%)
  Pallas kernels  15.8 us (15%)
    ppermute x36, waiting for transfers between devices, swapped(): lax.ppermute(value, axis, [(source, source ^ bit) for source in range(cou...  46.7 us
    ppermute x36, starting transfers between devices, swapped(): lax.ppermute(value, axis, [(source, source ^ bit) for source in range(cou...  37.9 us
    pallas_call x11, Pallas kernels, call(): pl.pallas_call(kernel, out_shape=out, in_specs=specs, out_specs=vmem, scr...  9.99 us
    pallas_call x3, Pallas kernels, copier(): pl.pallas_call(kernel, out_shape=[pltpu.VMEM(shape, dtype) for shape, dty...  5.81 us
    ppermute x1, starting transfers between devices, passed_along(): lax.ppermute(value, axis, [(source, source + steps) for source in range(l...  3.2 us
  transfers between devices with their start and end apart: 37, of which 10 were waited for; matrix products, arithmetic and copies ran while one was open for 0% of the time, Pallas kernels for 12%

profile of v1, /device:TPU:9, one launch (start us, length us, event | category | flops | bytes accessed | tf_op | source)
XLA Modules:
  0.0 103.8 jit_solution(11651086421752663159)
XLA Ops:
  0.0 1.8 %shard_map.156 = (bf16[272,128]{1,0:T(8,128)(2,1)S(1)}, s32[1,256]{1,0:T(1,128)}, bf16[256,512]{1,0:T(8,128)(2,1)S(1)}, bf16[256,512]{1,0:T(8,128)(2,1)S(1)}, bf16[256,512]{1,0:T(8,128)(2,1)S(1)}) custom-call(s32[1,256]{1,0:T(1,128)} %bitcast.17, bf16[256,128]{1,0:T(8,128)(2,1)} %k_hbm.1, bf16[256,128]{1,0:T(8,128)(2,1)} %v_hbm.1, bf16[256,2048]{1,0:T(8,128)(2,1)} %weight_hbm.1), custom_call_target="tpu_custom_call" | custom-call | tf_op jit(solution)/shard_map/pallas_call | solution.py:229
  1.8 3.2 %collective-permute-start = (bf16[272,128]{1,0:T(8,128)(2,1)S(1)}, bf16[272,128]{1,0:T(8,128)(2,1)S(1)}, u32[]{:S(2)}, u32[]{:S(2)}) collective-permute-start(bf16[272,128]{1,0:T(8,128)(2,1)S(1)} %get-tuple-element.33), channel_id=1, source_target_pairs={{0,4},{4,8},{8,12},{1,5},{5,9},{9,13},{2,6},{6,10},{10,14},{3,7},{... | collective-permute-start | bytes 208904 | tf_op jit(solution)/shard_map/ppermute | solution.py:21
  5.0 1.0 collective-permute-start.4
  6.0 1.2 %collective-permute-start.5 = (bf16[256,512]{1,0:T(8,128)(2,1)S(1)}, bf16[256,512]{1,0:T(8,128)(2,1)S(1)}, u32[]{:S(2)}, u32[]{:S(2)}) collective-permute-start(bf16[256,512]{1,0:T(8,128)(2,1)S(1)} %get-tuple-element.36), channel_id=1, source_target_pairs={{0,2},{1,3},{2,0},{3,1},{4,6},{5,7},{6,4},{7,5},{8,10},{9,11},{10,... | collective-permute-start | bytes 786440 | tf_op jit(solution)/shard_map/ppermute | solution.py:36
  7.2 0.5 collective-permute-start.6
  7.7 1.1 %shard_map.155 = (bf16[256,512]{1,0:T(8,128)(2,1)S(1)}, bf16[256,512]{1,0:T(8,128)(2,1)S(1)}, s32[1,256]{1,0:T(1,128)S(1)}, bf16[256,256]{1,0:T(8,128)(2,1)S(1)}...) custom-call(bf16[256,2048]{1,0:T(8,128)(2,1)} %refs_0_.1, bf16[256,2048]{1,0:T(8,128)(2,1)} %weight_hbm.1, ...), custom_call_target="tpu_custom_call" | custom-call | tf_op jit(solution)/shard_map/pallas_call | solution.py:229
  8.9 0.0 collective-permute-done.halo_ref
  8.9 2.0 %shard_map.157.refs_0_ = bf16[256,256]{1,0:T(8,128)(2,1)S(1)} custom-call(f32[4]{0:T(128)} %sink_hbm.1, s32[1,256]{1,0:T(1,128)S(1)} %get-tuple-element.29.row_ref, bf16[256,256]{1,0:T(8,128)(2,1)S(1)} %get-tuple-element.30.q_ref, bf16[256,128]{1,0:T(8,128)(2,1)S(1)} %get-tuple-element.31.k_ref, bf16[256,128]{1,0:T(8,128)(2,1)S(1)} %get-tuple-element.32.v_ref, ...), custom_call_target="tpu_custom_call" | custom-call | tf_op jit(solution)/shard_map/pallas_call | solution.py:217
  10.9 1.3 %collective-permute-start.2 = (bf16[256,256]{1,0:T(8,128)(2,1)S(1)}, bf16[256,256]{1,0:T(8,128)(2,1)S(1)}, u32[]{:S(2)}, u32[]{:S(2)}) collective-permute-start(bf16[256,256]{1,0:T(8,128)(2,1)S(1)} %shard_map.157.refs_0_), channel_id=1, source_target_pairs={{0,2},{1,3},{2,0},{3,1},{4,6},{5,7},{6,4},{7,5},{8,10},{9,11},{10,... | collective-permute-start | bytes 393224 | tf_op jit(solution)/shard_map/ppermute | solution.py:36
  12.2 0.4 collective-permute-start.1
  12.6 9.6 %collective-permute-done.2.refs_2_ = bf16[256,256]{1,0:T(8,128)(2,1)S(1)} collective-permute-done((bf16[256,256]{1,0:T(8,128)(2,1)S(1)}, bf16[256,256]{1,0:T(8,128)(2,1)S(1)}, u32[]{:S(2)}, u32[]{:S(2)}) %collective-permute-start.2) | collective-permute-done | bytes 131104 | tf_op jit(solution)/shard_map/ppermute | solution.py:36
  22.2 0.9 collective-permute-start.3
  23.2 0.0 collective-permute-done.6.refs_7_
  23.2 1.0 collective-permute-done.3.refs_3_
  24.2 0.4 shard_map.158.refs_0_.updated_ref
  24.6 0.2 collective-permute-start.21
  24.8 2.4 %collective-permute-start.13 = (bf16[256,512]{1,0:T(8,128)(2,1)S(1)}, bf16[256,512]{1,0:T(8,128)(2,1)S(1)}, u32[]{:S(2)}, u32[]{:S(2)}) collective-permute-start(bf16[256,512]{1,0:T(8,128)(2,1)S(1)} %shard_map.158.refs_0_.updated_ref), channel_id=1, source_target_pairs={{0,4},{4,0},{8,12},{12,8},{1,5},{5,1},{9,13},{13,9},{2,6},{6,2},{1... | collective-permute-start | bytes 786440 | tf_op jit(solution)/shard_map/ppermute | solution.py:36
  27.1 1.2 %collective-permute-start.8 = (bf16[256,512]{1,0:T(8,128)(2,1)S(1)}, bf16[256,512]{1,0:T(8,128)(2,1)S(1)}, u32[]{:S(2)}, u32[]{:S(2)}) collective-permute-start(bf16[256,512]{1,0:T(8,128)(2,1)S(1)} %shard_map.158.refs_0_.updated_ref), channel_id=1, source_target_pairs={{0,2},{1,3},{2,0},{3,1},{4,6},{5,7},{6,4},{7,5},{8,10},{9,11},{10,... | collective-permute-start | bytes 786440 | tf_op jit(solution)/shard_map/ppermute | solution.py:36
  28.4 7.3 %collective-permute-done.21.refs_0_ = bf16[256,512]{1,0:T(8,128)(2,1)S(1)} collective-permute-done((bf16[256,512]{1,0:T(8,128)(2,1)S(1)}, bf16[256,512]{1,0:T(8,128)(2,1)S(1)}, u32[]{:S(2)}, u32[]{:S(2)}) %collective-permute-start.21) | collective-permute-done | bytes 262176 | tf_op jit(solution)/shard_map/ppermute | solution.py:36
  35.7 1.2 %collective-permute-start.23 = (bf16[256,512]{1,0:T(8,128)(2,1)S(1)}, bf16[256,512]{1,0:T(8,128)(2,1)S(1)}, u32[]{:S(2)}, u32[]{:S(2)}) collective-permute-start(bf16[256,512]{1,0:T(8,128)(2,1)S(1)} %collective-permute-done.21.refs_0_), channel_id=1, source_target_pairs={{0,2},{1,3},{2,0},{3,1},{4,6},{5,7},{6,4},{7,5},{8,10},{9,11},{10,... | collective-permute-start | bytes 786440 | tf_op jit(solution)/shard_map/ppermute | solution.py:36
  36.9 1.5 %collective-permute-start.7 = (bf16[256,512]{1,0:T(8,128)(2,1)S(1)}, bf16[256,512]{1,0:T(8,128)(2,1)S(1)}, u32[]{:S(2)}, u32[]{:S(2)}) collective-permute-start(bf16[256,512]{1,0:T(8,128)(2,1)S(1)} %shard_map.158.refs_0_.updated_ref), channel_id=1, source_target_pairs={{0,1},{1,0},{2,3},{3,2},{4,5},{5,4},{6,7},{7,6},{8,9},{9,8},{10,11... | collective-permute-start | bytes 786440 | tf_op jit(solution)/shard_map/ppermute | solution.py:36
  38.4 3.3 %collective-permute-start.29 = (bf16[256,512]{1,0:T(8,128)(2,1)S(1)}, bf16[256,512]{1,0:T(8,128)(2,1)S(1)}, u32[]{:S(2)}, u32[]{:S(2)}) collective-permute-start(bf16[256,512]{1,0:T(8,128)(2,1)S(1)} %collective-permute-done.21.refs_0_), channel_id=1, source_target_pairs={{0,4},{4,0},{8,12},{12,8},{1,5},{5,1},{9,13},{13,9},{2,6},{6,2},{1... | collective-permute-start | bytes 786440 | tf_op jit(solution)/shard_map/ppermute | solution.py:36
  41.7 0.0 collective-permute-done.13.refs_0_
  41.7 0.3 collective-permute-start.22
  42.0 0.3 collective-permute-start.15
  42.2 0.1 collective-permute-done.23.refs_2_
  42.3 3.1 %collective-permute-start.31 = (bf16[256,512]{1,0:T(8,128)(2,1)S(1)}, bf16[256,512]{1,0:T(8,128)(2,1)S(1)}, u32[]{:S(2)}, u32[]{:S(2)}) collective-permute-start(bf16[256,512]{1,0:T(8,128)(2,1)S(1)} %collective-permute-done.23.refs_2_), channel_id=1, source_target_pairs={{0,4},{4,0},{8,12},{12,8},{1,5},{5,1},{9,13},{13,9},{2,6},{6,2},{1... | collective-permute-start | bytes 786440 | tf_op jit(solution)/shard_map/ppermute | solution.py:36
  45.5 4.1 %collective-permute-start.24 = (bf16[256,512]{1,0:T(8,128)(2,1)S(1)}, bf16[256,512]{1,0:T(8,128)(2,1)S(1)}, u32[]{:S(2)}, u32[]{:S(2)}) collective-permute-start(bf16[256,512]{1,0:T(8,128)(2,1)S(1)} %collective-permute-done.23.refs_2_), channel_id=1, source_target_pairs={{0,1},{1,0},{2,3},{3,2},{4,5},{5,4},{6,7},{7,6},{8,9},{9,8},{10,11... | collective-permute-start | bytes 786440 | tf_op jit(solution)/shard_map/ppermute | solution.py:36
  49.6 0.1 collective-permute-start.9
  49.7 0.4 collective-permute-start.14
  50.2 0.5 collective-permute-start.16
  50.7 1.2 %collective-permute-done.31.refs_2_ = bf16[256,512]{1,0:T(8,128)(2,1)S(1)} collective-permute-done((bf16[256,512]{1,0:T(8,128)(2,1)S(1)}, bf16[256,512]{1,0:T(8,128)(2,1)S(1)}, u32[]{:S(2)}, u32[]{:S(2)}) %collective-permute-start.31) | collective-permute-done | bytes 262176 | tf_op jit(solution)/shard_map/ppermute | solution.py:36
  51.9 2.6 %collective-permute-start.30 = (bf16[256,512]{1,0:T(8,128)(2,1)S(1)}, bf16[256,512]{1,0:T(8,128)(2,1)S(1)}, u32[]{:S(2)}, u32[]{:S(2)}) collective-permute-start(bf16[256,512]{1,0:T(8,128)(2,1)S(1)} %collective-permute-done.29.refs_0_), channel_id=1, source_target_pairs={{0,1},{1,0},{2,3},{3,2},{4,5},{5,4},{6,7},{7,6},{8,9},{9,8},{10,11... | collective-permute-start | bytes 786440 | tf_op jit(solution)/shard_map/ppermute | solution.py:36
  54.5 0.0 collective-permute-start.32
  54.5 2.9 %shard_map.154 = (f32[4,1,512]{2,1,0:T(1,128)S(1)}, bf16[4,512,256]{2,1,0:T(8,128)(2,1)S(1)}, bf16[4,512,256]{2,1,0:T(8,128)(2,1)S(1)}, bf16[4,512,256]{2,1,0:T(...) custom-call(f32[4,1,512]{2,1,0:T(1,128)} %bitcast.16, ...), custom_call_target="tpu_custom_call" | custom-call | tf_op jit(solution)/shard_map/pallas_call | solution.py:229
  57.4 1.0 shard_map.163.refs_0_
  58.4 0.7 collective-permute-start.26
  59.1 1.5 %shard_map.159.refs_0_ = bf16[256,512]{1,0:T(8,128)(2,1)S(1)} custom-call(f32[4,1,512]{2,1,0:T(1,128)S(1)} %get-tuple-element.38.gain_ref, bf16[256,512]{1,0:T(8,128)(2,1)S(1)} %shard_map.158.refs_0_.updated_ref, bf16[256,512]{1,0:T(8,128)(2,1)S(1)} %collective-permute-done.7.refs_1_, bf16[256,512]{1,0:T(8,128)(2,1)S(1)} %collective-permute-done.8.refs_2_, ...), custom_call_target="tpu_custom_call" | custom-call | tf_op jit(solution)/shard_map/pallas_call | solution.py:217
  60.7 0.9 collective-permute-start.11
  61.6 1.1 %collective-permute-start.25 = (bf16[256,256]{1,0:T(8,128)(2,1)S(1)}, bf16[256,256]{1,0:T(8,128)(2,1)S(1)}, u32[]{:S(2)}, u32[]{:S(2)}) collective-permute-start(bf16[256,256]{1,0:T(8,128)(2,1)S(1)} %shard_map.163.refs_0_), channel_id=1, source_target_pairs={{0,1},{1,0},{2,3},{3,2},{4,5},{5,4},{6,7},{7,6},{8,9},{9,8},{10,11... | collective-permute-start | bytes 393224 | tf_op jit(solution)/shard_map/ppermute | solution.py:36
  62.7 1.0 shard_map.161.refs_0_
  63.6 0.7 collective-permute-start.18
  64.3 0.6 collective-permute-start.27
  65.0 1.0 shard_map.165.refs_0_
  65.9 0.6 collective-permute-start.34
  66.5 0.5 collective-permute-start.17
  67.0 4.7 %collective-permute-done.18.refs_2_ = bf16[256,256]{1,0:T(8,128)(2,1)S(1)} collective-permute-done((bf16[256,256]{1,0:T(8,128)(2,1)S(1)}, bf16[256,256]{1,0:T(8,128)(2,1)S(1)}, u32[]{:S(2)}, u32[]{:S(2)}) %collective-permute-start.18) | collective-permute-done | bytes 131104 | tf_op jit(solution)/shard_map/ppermute | solution.py:36
  71.7 1.8 %collective-permute-start.19 = (bf16[256,256]{1,0:T(8,128)(2,1)S(1)}, bf16[256,256]{1,0:T(8,128)(2,1)S(1)}, u32[]{:S(2)}, u32[]{:S(2)}) collective-permute-start(bf16[256,256]{1,0:T(8,128)(2,1)S(1)} %collective-permute-done.18.refs_2_), channel_id=1, source_target_pairs={{0,1},{1,0},{2,3},{3,2},{4,5},{5,4},{6,7},{7,6},{8,9},{9,8},{10,11... | collective-permute-start | bytes 393224 | tf_op jit(solution)/shard_map/ppermute | solution.py:36
  73.5 0.0 collective-permute-start.33
  73.5 1.0 collective-permute-done.34.refs_2_
  74.5 1.1 %collective-permute-start.35 = (bf16[256,256]{1,0:T(8,128)(2,1)S(1)}, bf16[256,256]{1,0:T(8,128)(2,1)S(1)}, u32[]{:S(2)}, u32[]{:S(2)}) collective-permute-start(bf16[256,256]{1,0:T(8,128)(2,1)S(1)} %collective-permute-done.34.refs_2_), channel_id=1, source_target_pairs={{0,1},{1,0},{2,3},{3,2},{4,5},{5,4},{6,7},{7,6},{8,9},{9,8},{10,11... | collective-permute-start | bytes 393224 | tf_op jit(solution)/shard_map/ppermute | solution.py:36
  75.6 0.4 shard_map.164
  76.1 0.1 collective-permute-start.10
  76.2 0.5 collective-permute-start.12
  76.7 1.3 %collective-permute-start.28 = (bf16[256,512]{1,0:T(8,128)(2,1)S(1)}, bf16[256,512]{1,0:T(8,128)(2,1)S(1)}, u32[]{:S(2)}, u32[]{:S(2)}) collective-permute-start(bf16[256,512]{1,0:T(8,128)(2,1)S(1)} %shard_map.164), channel_id=1, source_target_pairs={{0,8},{4,12},{8,0},{12,4},{1,9},{5,13},{9,1},{13,5},{2,10},{6,14},... | collective-permute-start | bytes 786440 | tf_op jit(solution)/shard_map/ppermute | solution.py:36
  78.0 0.4 shard_map.162
  78.4 0.2 collective-permute-start.20
  78.7 0.4 shard_map.166
  79.1 1.3 %collective-permute-start.36 = (bf16[256,512]{1,0:T(8,128)(2,1)S(1)}, bf16[256,512]{1,0:T(8,128)(2,1)S(1)}, u32[]{:S(2)}, u32[]{:S(2)}) collective-permute-start(bf16[256,512]{1,0:T(8,128)(2,1)S(1)} %shard_map.166), channel_id=1, source_target_pairs={{0,12},{4,8},{8,4},{12,0},{1,13},{5,9},{9,5},{13,1},{2,14},{6,10},... | collective-permute-start | bytes 786440 | tf_op jit(solution)/shard_map/ppermute | solution.py:36
  80.4 0.7 shard_map.160.base_ref
  81.1 8.4 %collective-permute-done.28.refs_1_ = bf16[256,512]{1,0:T(8,128)(2,1)S(1)} collective-permute-done((bf16[256,512]{1,0:T(8,128)(2,1)S(1)}, bf16[256,512]{1,0:T(8,128)(2,1)S(1)}, u32[]{:S(2)}, u32[]{:S(2)}) %collective-permute-start.28) | collective-permute-done | bytes 262176 | tf_op jit(solution)/shard_map/ppermute | solution.py:36
  89.5 0.8 collective-permute-done.20.refs_0_
  90.3 12.4 %collective-permute-done.36.refs_2_ = bf16[256,512]{1,0:T(8,128)(2,1)S(1)} collective-permute-done((bf16[256,512]{1,0:T(8,128)(2,1)S(1)}, bf16[256,512]{1,0:T(8,128)(2,1)S(1)}, u32[]{:S(2)}, u32[]{:S(2)}) %collective-permute-start.36) | collective-permute-done | bytes 262176 | tf_op jit(solution)/shard_map/ppermute | solution.py:36
  102.7 1.1 %shard_map.167 = bf16[256,512]{1,0:T(8,128)(2,1)} custom-call(s32[2,256]{1,0:T(2,128)S(1)} %get-tuple-element.24.routes_ref, f32[2,256]{1,0:T(2,128)S(1)} %get-tuple-element.25.weight_ref, f32[256,512]{1,0:T(8,128)S(1)} %shard_map.160.base_ref, bf16[256,512]{1,0:T(8,128)(2,1)S(1)} %collective-permute-done.20.refs_0_, ...), custom_call_target="tpu_custom_call" | custom-call | tf_op jit(solution)/shard_map/pallas_call | solution.py:217
  (24 shorter events, 0.1 us)
Async XLA Ops:
  1.8 7.1 %collective-permute-start = (bf16[272,128]{1,0:T(8,128)(2,1)S(1)}, bf16[272,128]{1,0:T(8,128)(2,1)S(1)}, u32[]{:S(2)}, u32[]{:S(2)}) collective-permute-start(bf16[272,128]{1,0:T(8,128)(2,1)S(1)} %get-tuple-element.33), channel_id=1, source_target_pairs={{0,4},{4,8},{8,12},{1,5},{5,9},{9,13},{2,6},{6,10},{10,14},{3,7},{... | collective-permute-start | bytes 208904 | tf_op jit(solution)/shard_map/ppermute | solution.py:21
  5.0 18.2 %collective-permute-start.4 = (bf16[256,512]{1,0:T(8,128)(2,1)S(1)}, bf16[256,512]{1,0:T(8,128)(2,1)S(1)}, u32[]{:S(2)}, u32[]{:S(2)}) collective-permute-start(bf16[256,512]{1,0:T(8,128)(2,1)S(1)} %get-tuple-element.35), channel_id=1, source_target_pairs={{0,1},{1,0},{2,3},{3,2},{4,5},{5,4},{6,7},{7,6},{8,9},{9,8},{10,11... | collective-permute-start | bytes 786440 | tf_op jit(solution)/shard_map/ppermute | solution.py:36
  6.0 17.2 %collective-permute-start.5 = (bf16[256,512]{1,0:T(8,128)(2,1)S(1)}, bf16[256,512]{1,0:T(8,128)(2,1)S(1)}, u32[]{:S(2)}, u32[]{:S(2)}) collective-permute-start(bf16[256,512]{1,0:T(8,128)(2,1)S(1)} %get-tuple-element.36), channel_id=1, source_target_pairs={{0,2},{1,3},{2,0},{3,1},{4,6},{5,7},{6,4},{7,5},{8,10},{9,11},{10,... | collective-permute-start | bytes 786440 | tf_op jit(solution)/shard_map/ppermute | solution.py:36
  7.2 16.0 %collective-permute-start.6 = (bf16[256,512]{1,0:T(8,128)(2,1)S(1)}, bf16[256,512]{1,0:T(8,128)(2,1)S(1)}, u32[]{:S(2)}, u32[]{:S(2)}) collective-permute-start(bf16[256,512]{1,0:T(8,128)(2,1)S(1)} %get-tuple-element.37), channel_id=1, source_target_pairs={{0,3},{1,2},{2,1},{3,0},{4,7},{5,6},{6,5},{7,4},{8,11},{9,10},{10,... | collective-permute-start | bytes 786440 | tf_op jit(solution)/shard_map/ppermute | solution.py:36
  10.9 11.3 %collective-permute-start.2 = (bf16[256,256]{1,0:T(8,128)(2,1)S(1)}, bf16[256,256]{1,0:T(8,128)(2,1)S(1)}, u32[]{:S(2)}, u32[]{:S(2)}) collective-permute-start(bf16[256,256]{1,0:T(8,128)(2,1)S(1)} %shard_map.157.refs_0_), channel_id=1, source_target_pairs={{0,2},{1,3},{2,0},{3,1},{4,6},{5,7},{6,4},{7,5},{8,10},{9,11},{10,... | collective-permute-start | bytes 393224 | tf_op jit(solution)/shard_map/ppermute | solution.py:36
  12.2 11.0 %collective-permute-start.1 = (bf16[256,256]{1,0:T(8,128)(2,1)S(1)}, bf16[256,256]{1,0:T(8,128)(2,1)S(1)}, u32[]{:S(2)}, u32[]{:S(2)}) collective-permute-start(bf16[256,256]{1,0:T(8,128)(2,1)S(1)} %shard_map.157.refs_0_), channel_id=1, source_target_pairs={{0,1},{1,0},{2,3},{3,2},{4,5},{5,4},{6,7},{7,6},{8,9},{9,8},{10,11... | collective-permute-start | bytes 393224 | tf_op jit(solution)/shard_map/ppermute | solution.py:36
  22.2 1.9 %collective-permute-start.3 = (bf16[256,256]{1,0:T(8,128)(2,1)S(1)}, bf16[256,256]{1,0:T(8,128)(2,1)S(1)}, u32[]{:S(2)}, u32[]{:S(2)}) collective-permute-start(bf16[256,256]{1,0:T(8,128)(2,1)S(1)} %collective-permute-done.2.refs_2_), channel_id=1, source_target_pairs={{0,1},{1,0},{2,3},{3,2},{4,5},{5,4},{6,7},{7,6},{8,9},{9,8},{10,11... | collective-permute-start | bytes 393224 | tf_op jit(solution)/shard_map/ppermute | solution.py:36
  24.6 11.1 %collective-permute-start.21 = (bf16[256,512]{1,0:T(8,128)(2,1)S(1)}, bf16[256,512]{1,0:T(8,128)(2,1)S(1)}, u32[]{:S(2)}, u32[]{:S(2)}) collective-permute-start(bf16[256,512]{1,0:T(8,128)(2,1)S(1)} %shard_map.158.refs_0_.updated_ref), channel_id=1, source_target_pairs={{0,8},{4,12},{8,0},{12,4},{1,9},{5,13},{9,1},{13,5},{2,10},{6,14},... | collective-permute-start | bytes 786440 | tf_op jit(solution)/shard_map/ppermute | solution.py:36
  24.8 16.9 %collective-permute-start.13 = (bf16[256,512]{1,0:T(8,128)(2,1)S(1)}, bf16[256,512]{1,0:T(8,128)(2,1)S(1)}, u32[]{:S(2)}, u32[]{:S(2)}) collective-permute-start(bf16[256,512]{1,0:T(8,128)(2,1)S(1)} %shard_map.158.refs_0_.updated_ref), channel_id=1, source_target_pairs={{0,4},{4,0},{8,12},{12,8},{1,5},{5,1},{9,13},{13,9},{2,6},{6,2},{1... | collective-permute-start | bytes 786440 | tf_op jit(solution)/shard_map/ppermute | solution.py:36
  27.1 14.8 %collective-permute-start.8 = (bf16[256,512]{1,0:T(8,128)(2,1)S(1)}, bf16[256,512]{1,0:T(8,128)(2,1)S(1)}, u32[]{:S(2)}, u32[]{:S(2)}) collective-permute-start(bf16[256,512]{1,0:T(8,128)(2,1)S(1)} %shard_map.158.refs_0_.updated_ref), channel_id=1, source_target_pairs={{0,2},{1,3},{2,0},{3,1},{4,6},{5,7},{6,4},{7,5},{8,10},{9,11},{10,... | collective-permute-start | bytes 786440 | tf_op jit(solution)/shard_map/ppermute | solution.py:36
  35.7 6.6 %collective-permute-start.23 = (bf16[256,512]{1,0:T(8,128)(2,1)S(1)}, bf16[256,512]{1,0:T(8,128)(2,1)S(1)}, u32[]{:S(2)}, u32[]{:S(2)}) collective-permute-start(bf16[256,512]{1,0:T(8,128)(2,1)S(1)} %collective-permute-done.21.refs_0_), channel_id=1, source_target_pairs={{0,2},{1,3},{2,0},{3,1},{4,6},{5,7},{6,4},{7,5},{8,10},{9,11},{10,... | collective-permute-start | bytes 786440 | tf_op jit(solution)/shard_map/ppermute | solution.py:36
  36.9 8.6 %collective-permute-start.7 = (bf16[256,512]{1,0:T(8,128)(2,1)S(1)}, bf16[256,512]{1,0:T(8,128)(2,1)S(1)}, u32[]{:S(2)}, u32[]{:S(2)}) collective-permute-start(bf16[256,512]{1,0:T(8,128)(2,1)S(1)} %shard_map.158.refs_0_.updated_ref), channel_id=1, source_target_pairs={{0,1},{1,0},{2,3},{3,2},{4,5},{5,4},{6,7},{7,6},{8,9},{9,8},{10,11... | collective-permute-start | bytes 786440 | tf_op jit(solution)/shard_map/ppermute | solution.py:36
  38.4 11.2 %collective-permute-start.29 = (bf16[256,512]{1,0:T(8,128)(2,1)S(1)}, bf16[256,512]{1,0:T(8,128)(2,1)S(1)}, u32[]{:S(2)}, u32[]{:S(2)}) collective-permute-start(bf16[256,512]{1,0:T(8,128)(2,1)S(1)} %collective-permute-done.21.refs_0_), channel_id=1, source_target_pairs={{0,4},{4,0},{8,12},{12,8},{1,5},{5,1},{9,13},{13,9},{2,6},{6,2},{1... | collective-permute-start | bytes 786440 | tf_op jit(solution)/shard_map/ppermute | solution.py:36
  41.7 8.0 %collective-permute-start.22 = (bf16[256,512]{1,0:T(8,128)(2,1)S(1)}, bf16[256,512]{1,0:T(8,128)(2,1)S(1)}, u32[]{:S(2)}, u32[]{:S(2)}) collective-permute-start(bf16[256,512]{1,0:T(8,128)(2,1)S(1)} %collective-permute-done.21.refs_0_), channel_id=1, source_target_pairs={{0,1},{1,0},{2,3},{3,2},{4,5},{5,4},{6,7},{7,6},{8,9},{9,8},{10,11... | collective-permute-start | bytes 786440 | tf_op jit(solution)/shard_map/ppermute | solution.py:36
  42.0 8.2 %collective-permute-start.15 = (bf16[256,512]{1,0:T(8,128)(2,1)S(1)}, bf16[256,512]{1,0:T(8,128)(2,1)S(1)}, u32[]{:S(2)}, u32[]{:S(2)}) collective-permute-start(bf16[256,512]{1,0:T(8,128)(2,1)S(1)} %collective-permute-done.13.refs_0_), channel_id=1, source_target_pairs={{0,2},{1,3},{2,0},{3,1},{4,6},{5,7},{6,4},{7,5},{8,10},{9,11},{10,... | collective-permute-start | bytes 786440 | tf_op jit(solution)/shard_map/ppermute | solution.py:36
  42.3 9.5 %collective-permute-start.31 = (bf16[256,512]{1,0:T(8,128)(2,1)S(1)}, bf16[256,512]{1,0:T(8,128)(2,1)S(1)}, u32[]{:S(2)}, u32[]{:S(2)}) collective-permute-start(bf16[256,512]{1,0:T(8,128)(2,1)S(1)} %collective-permute-done.23.refs_2_), channel_id=1, source_target_pairs={{0,4},{4,0},{8,12},{12,8},{1,5},{5,1},{9,13},{13,9},{2,6},{6,2},{1... | collective-permute-start | bytes 786440 | tf_op jit(solution)/shard_map/ppermute | solution.py:36
  45.5 9.1 %collective-permute-start.24 = (bf16[256,512]{1,0:T(8,128)(2,1)S(1)}, bf16[256,512]{1,0:T(8,128)(2,1)S(1)}, u32[]{:S(2)}, u32[]{:S(2)}) collective-permute-start(bf16[256,512]{1,0:T(8,128)(2,1)S(1)} %collective-permute-done.23.refs_2_), channel_id=1, source_target_pairs={{0,1},{1,0},{2,3},{3,2},{4,5},{5,4},{6,7},{7,6},{8,9},{9,8},{10,11... | collective-permute-start | bytes 786440 | tf_op jit(solution)/shard_map/ppermute | solution.py:36
  49.6 8.8 %collective-permute-start.9 = (bf16[256,512]{1,0:T(8,128)(2,1)S(1)}, bf16[256,512]{1,0:T(8,128)(2,1)S(1)}, u32[]{:S(2)}, u32[]{:S(2)}) collective-permute-start(bf16[256,512]{1,0:T(8,128)(2,1)S(1)} %collective-permute-done.8.refs_2_), channel_id=1, source_target_pairs={{0,1},{1,0},{2,3},{3,2},{4,5},{5,4},{6,7},{7,6},{8,9},{9,8},{10,11... | collective-permute-start | bytes 786440 | tf_op jit(solution)/shard_map/ppermute | solution.py:36
  49.7 11.0 %collective-permute-start.14 = (bf16[256,512]{1,0:T(8,128)(2,1)S(1)}, bf16[256,512]{1,0:T(8,128)(2,1)S(1)}, u32[]{:S(2)}, u32[]{:S(2)}) collective-permute-start(bf16[256,512]{1,0:T(8,128)(2,1)S(1)} %collective-permute-done.13.refs_0_), channel_id=1, source_target_pairs={{0,1},{1,0},{2,3},{3,2},{4,5},{5,4},{6,7},{7,6},{8,9},{9,8},{10,11... | collective-permute-start | bytes 786440 | tf_op jit(solution)/shard_map/ppermute | solution.py:36
  50.2 11.4 %collective-permute-start.16 = (bf16[256,512]{1,0:T(8,128)(2,1)S(1)}, bf16[256,512]{1,0:T(8,128)(2,1)S(1)}, u32[]{:S(2)}, u32[]{:S(2)}) collective-permute-start(bf16[256,512]{1,0:T(8,128)(2,1)S(1)} %collective-permute-done.15.refs_2_), channel_id=1, source_target_pairs={{0,1},{1,0},{2,3},{3,2},{4,5},{5,4},{6,7},{7,6},{8,9},{9,8},{10,11... | collective-permute-start | bytes 786440 | tf_op jit(solution)/shard_map/ppermute | solution.py:36
  51.9 11.7 %collective-permute-start.30 = (bf16[256,512]{1,0:T(8,128)(2,1)S(1)}, bf16[256,512]{1,0:T(8,128)(2,1)S(1)}, u32[]{:S(2)}, u32[]{:S(2)}) collective-permute-start(bf16[256,512]{1,0:T(8,128)(2,1)S(1)} %collective-permute-done.29.refs_0_), channel_id=1, source_target_pairs={{0,1},{1,0},{2,3},{3,2},{4,5},{5,4},{6,7},{7,6},{8,9},{9,8},{10,11... | collective-permute-start | bytes 786440 | tf_op jit(solution)/shard_map/ppermute | solution.py:36
  54.5 10.4 %collective-permute-start.32 = (bf16[256,512]{1,0:T(8,128)(2,1)S(1)}, bf16[256,512]{1,0:T(8,128)(2,1)S(1)}, u32[]{:S(2)}, u32[]{:S(2)}) collective-permute-start(bf16[256,512]{1,0:T(8,128)(2,1)S(1)} %collective-permute-done.31.refs_2_), channel_id=1, source_target_pairs={{0,1},{1,0},{2,3},{3,2},{4,5},{5,4},{6,7},{7,6},{8,9},{9,8},{10,11... | collective-permute-start | bytes 786440 | tf_op jit(solution)/shard_map/ppermute | solution.py:36
  58.4 5.9 %collective-permute-start.26 = (bf16[256,256]{1,0:T(8,128)(2,1)S(1)}, bf16[256,256]{1,0:T(8,128)(2,1)S(1)}, u32[]{:S(2)}, u32[]{:S(2)}) collective-permute-start(bf16[256,256]{1,0:T(8,128)(2,1)S(1)} %shard_map.163.refs_0_), channel_id=1, source_target_pairs={{0,2},{1,3},{2,0},{3,1},{4,6},{5,7},{6,4},{7,5},{8,10},{9,11},{10,... | collective-permute-start | bytes 393224 | tf_op jit(solution)/shard_map/ppermute | solution.py:36
  60.7 15.4 %collective-permute-start.11 = (bf16[256,512]{1,0:T(8,128)(2,1)S(1)}, bf16[256,512]{1,0:T(8,128)(2,1)S(1)}, u32[]{:S(2)}, u32[]{:S(2)}) collective-permute-start(bf16[256,512]{1,0:T(8,128)(2,1)S(1)} %shard_map.159.refs_0_), channel_id=1, source_target_pairs={{0,2},{1,3},{2,0},{3,1},{4,6},{5,7},{6,4},{7,5},{8,10},{9,11},{10,... | collective-permute-start | bytes 786440 | tf_op jit(solution)/shard_map/ppermute | solution.py:36
  61.6 4.9 %collective-permute-start.25 = (bf16[256,256]{1,0:T(8,128)(2,1)S(1)}, bf16[256,256]{1,0:T(8,128)(2,1)S(1)}, u32[]{:S(2)}, u32[]{:S(2)}) collective-permute-start(bf16[256,256]{1,0:T(8,128)(2,1)S(1)} %shard_map.163.refs_0_), channel_id=1, source_target_pairs={{0,1},{1,0},{2,3},{3,2},{4,5},{5,4},{6,7},{7,6},{8,9},{9,8},{10,11... | collective-permute-start | bytes 393224 | tf_op jit(solution)/shard_map/ppermute | solution.py:36
  63.6 8.1 %collective-permute-start.18 = (bf16[256,256]{1,0:T(8,128)(2,1)S(1)}, bf16[256,256]{1,0:T(8,128)(2,1)S(1)}, u32[]{:S(2)}, u32[]{:S(2)}) collective-permute-start(bf16[256,256]{1,0:T(8,128)(2,1)S(1)} %shard_map.161.refs_0_), channel_id=1, source_target_pairs={{0,2},{1,3},{2,0},{3,1},{4,6},{5,7},{6,4},{7,5},{8,10},{9,11},{10,... | collective-permute-start | bytes 393224 | tf_op jit(solution)/shard_map/ppermute | solution.py:36
  64.3 9.2 %collective-permute-start.27 = (bf16[256,256]{1,0:T(8,128)(2,1)S(1)}, bf16[256,256]{1,0:T(8,128)(2,1)S(1)}, u32[]{:S(2)}, u32[]{:S(2)}) collective-permute-start(bf16[256,256]{1,0:T(8,128)(2,1)S(1)} %collective-permute-done.26.refs_2_), channel_id=1, source_target_pairs={{0,1},{1,0},{2,3},{3,2},{4,5},{5,4},{6,7},{7,6},{8,9},{9,8},{10,11... | collective-permute-start | bytes 393224 | tf_op jit(solution)/shard_map/ppermute | solution.py:36
  65.9 8.6 %collective-permute-start.34 = (bf16[256,256]{1,0:T(8,128)(2,1)S(1)}, bf16[256,256]{1,0:T(8,128)(2,1)S(1)}, u32[]{:S(2)}, u32[]{:S(2)}) collective-permute-start(bf16[256,256]{1,0:T(8,128)(2,1)S(1)} %shard_map.165.refs_0_), channel_id=1, source_target_pairs={{0,2},{1,3},{2,0},{3,1},{4,6},{5,7},{6,4},{7,5},{8,10},{9,11},{10,... | collective-permute-start | bytes 393224 | tf_op jit(solution)/shard_map/ppermute | solution.py:36
  66.5 9.7 %collective-permute-start.17 = (bf16[256,256]{1,0:T(8,128)(2,1)S(1)}, bf16[256,256]{1,0:T(8,128)(2,1)S(1)}, u32[]{:S(2)}, u32[]{:S(2)}) collective-permute-start(bf16[256,256]{1,0:T(8,128)(2,1)S(1)} %shard_map.161.refs_0_), channel_id=1, source_target_pairs={{0,1},{1,0},{2,3},{3,2},{4,5},{5,4},{6,7},{7,6},{8,9},{9,8},{10,11... | collective-permute-start | bytes 393224 | tf_op jit(solution)/shard_map/ppermute | solution.py:36
  71.7 4.9 %collective-permute-start.19 = (bf16[256,256]{1,0:T(8,128)(2,1)S(1)}, bf16[256,256]{1,0:T(8,128)(2,1)S(1)}, u32[]{:S(2)}, u32[]{:S(2)}) collective-permute-start(bf16[256,256]{1,0:T(8,128)(2,1)S(1)} %collective-permute-done.18.refs_2_), channel_id=1, source_target_pairs={{0,1},{1,0},{2,3},{3,2},{4,5},{5,4},{6,7},{7,6},{8,9},{9,8},{10,11... | collective-permute-start | bytes 393224 | tf_op jit(solution)/shard_map/ppermute | solution.py:36
  73.5 4.9 %collective-permute-start.33 = (bf16[256,256]{1,0:T(8,128)(2,1)S(1)}, bf16[256,256]{1,0:T(8,128)(2,1)S(1)}, u32[]{:S(2)}, u32[]{:S(2)}) collective-permute-start(bf16[256,256]{1,0:T(8,128)(2,1)S(1)} %shard_map.165.refs_0_), channel_id=1, source_target_pairs={{0,1},{1,0},{2,3},{3,2},{4,5},{5,4},{6,7},{7,6},{8,9},{9,8},{10,11... | collective-permute-start | bytes 393224 | tf_op jit(solution)/shard_map/ppermute | solution.py:36
  74.5 4.1 %collective-permute-start.35 = (bf16[256,256]{1,0:T(8,128)(2,1)S(1)}, bf16[256,256]{1,0:T(8,128)(2,1)S(1)}, u32[]{:S(2)}, u32[]{:S(2)}) collective-permute-start(bf16[256,256]{1,0:T(8,128)(2,1)S(1)} %collective-permute-done.34.refs_2_), channel_id=1, source_target_pairs={{0,1},{1,0},{2,3},{3,2},{4,5},{5,4},{6,7},{7,6},{8,9},{9,8},{10,11... | collective-permute-start | bytes 393224 | tf_op jit(solution)/shard_map/ppermute | solution.py:36
  76.1 4.3 %collective-permute-start.10 = (bf16[256,512]{1,0:T(8,128)(2,1)S(1)}, bf16[256,512]{1,0:T(8,128)(2,1)S(1)}, u32[]{:S(2)}, u32[]{:S(2)}) collective-permute-start(bf16[256,512]{1,0:T(8,128)(2,1)S(1)} %shard_map.159.refs_0_), channel_id=1, source_target_pairs={{0,1},{1,0},{2,3},{3,2},{4,5},{5,4},{6,7},{7,6},{8,9},{9,8},{10,11... | collective-permute-start | bytes 786440 | tf_op jit(solution)/shard_map/ppermute | solution.py:36
  76.2 4.2 %collective-permute-start.12 = (bf16[256,512]{1,0:T(8,128)(2,1)S(1)}, bf16[256,512]{1,0:T(8,128)(2,1)S(1)}, u32[]{:S(2)}, u32[]{:S(2)}) collective-permute-start(bf16[256,512]{1,0:T(8,128)(2,1)S(1)} %collective-permute-done.11.refs_2_), channel_id=1, source_target_pairs={{0,1},{1,0},{2,3},{3,2},{4,5},{5,4},{6,7},{7,6},{8,9},{9,8},{10,11... | collective-permute-start | bytes 786440 | tf_op jit(solution)/shard_map/ppermute | solution.py:36
  76.7 12.8 %collective-permute-start.28 = (bf16[256,512]{1,0:T(8,128)(2,1)S(1)}, bf16[256,512]{1,0:T(8,128)(2,1)S(1)}, u32[]{:S(2)}, u32[]{:S(2)}) collective-permute-start(bf16[256,512]{1,0:T(8,128)(2,1)S(1)} %shard_map.164), channel_id=1, source_target_pairs={{0,8},{4,12},{8,0},{12,4},{1,9},{5,13},{9,1},{13,5},{2,10},{6,14},... | collective-permute-start | bytes 786440 | tf_op jit(solution)/shard_map/ppermute | solution.py:36
  78.4 11.8 %collective-permute-start.20 = (bf16[256,512]{1,0:T(8,128)(2,1)S(1)}, bf16[256,512]{1,0:T(8,128)(2,1)S(1)}, u32[]{:S(2)}, u32[]{:S(2)}) collective-permute-start(bf16[256,512]{1,0:T(8,128)(2,1)S(1)} %shard_map.162), channel_id=1, source_target_pairs={{0,4},{4,0},{8,12},{12,8},{1,5},{5,1},{9,13},{13,9},{2,6},{6,2},{1... | collective-permute-start | bytes 786440 | tf_op jit(solution)/shard_map/ppermute | solution.py:36
  79.1 23.6 %collective-permute-start.36 = (bf16[256,512]{1,0:T(8,128)(2,1)S(1)}, bf16[256,512]{1,0:T(8,128)(2,1)S(1)}, u32[]{:S(2)}, u32[]{:S(2)}) collective-permute-start(bf16[256,512]{1,0:T(8,128)(2,1)S(1)} %shard_map.166), channel_id=1, source_target_pairs={{0,12},{4,8},{8,4},{12,0},{1,13},{5,9},{9,5},{13,1},{2,14},{6,10},... | collective-permute-start | bytes 786440 | tf_op jit(solution)/shard_map/ppermute | solution.py:36
